TPU v7x, 512 devices: a whole 4x8x8 slice. The times are simulated.
512 devices in a mesh: sp: 64 (over z, y), tp: 4 (over x), dp: 2 (over core).
Axes of the slice: x: 4, y: 8, z: 8, core: 2. Of those that a mesh axis runs over, the one named last changes fastest.
Arguments:
- latent: bfloat16 [2, 8192, 2048], P('dp', ('sp', 'tp')), may hold values from -10 to 10
- condition: bfloat16 [2, 2048], P('dp'), may hold values from -6 to 6
- context: bfloat16 [2, 512, 2048], P('dp', 'sp'), may hold values from -6 to 6
- context_source: bfloat16 [2048], replicated, may hold values from -6 to 6
- mod_weight: bfloat16 [3, 2048, 2048], P(None, 'sp', 'tp'), may hold values from -0.125 to 0.125
- norm_gain: bfloat16 [2048], replicated, may hold values from 0.099609375 to 1.8984375
- w_x: bfloat16 [2048, 2048], P('dp', 'tp'), may hold values from -0.125 to 0.125
- w_b: bfloat16 [2048, 512], P('dp', 'tp'), may hold values from -0.125 to 0.125
- w_c: bfloat16 [2048, 512], P('dp', 'tp'), may hold values from -0.125 to 0.125
- w_z: bfloat16 [2048, 2048], P('dp', 'tp'), may hold values from -0.125 to 0.125
- w_dt: bfloat16 [2, 2048, 32], P(None, 'dp', 'tp'), may hold values from -0.125 to 0.125
- conv_x: bfloat16 [3, 2048], P(None, 'tp'), may hold values from -3.5 to 3.5
- conv_b: bfloat16 [3, 512], P(None, 'tp'), may hold values from -3.5 to 3.5
- conv_c: bfloat16 [3, 512], P(None, 'tp'), may hold values from -3.5 to 3.5
- decay_rate: float32 [2, 32], P(None, 'tp'), may hold values from 0 to 1, as said below
- out_gain: bfloat16 [2048], P('tp'), may hold values from 0.099609375 to 1.8984375
- w_out: bfloat16 [2048, 2048], P(('tp', 'dp')), may hold values from -0.125 to 0.125
Outputs:
- update: bfloat16 [2, 8192, 2048], P('dp', ('sp', 'tp'))
Inputs may be any that keep to these rules, and one draw needn't show every extreme that they name: `decay_rate`: positive rates.
All inputs are finite; a program needn't handle non-finite values.
Results may differ from a plain program's by a relative error of at most 0.014.
Values may be sent and summed in bfloat16 or wider, within the bound.
A program may use at most 128 MiB of HBM per device.

v0:
```python
import functools

import jax
import jax.numpy as jnp
from jax import lax
from jax.experimental import pallas as pl
from jax.experimental.pallas import tpu as pltpu
from jax.sharding import PartitionSpec as P

STATE = 128
LANES = 128
PAD = 16
EPSILON = 1e-06
MESH = pl.DeviceIdType.MESH
F32 = jnp.float32
BF16 = jnp.bfloat16


def silu(v):
    return v / (1.0 + jnp.exp(-v))


def softplus(v):
    return jnp.maximum(v, 0.0) + jnp.log1p(jnp.exp(-jnp.abs(v)))


def row_of(ref):
    return ref[...].astype(F32).reshape(1, ref.shape[0])


def dot(a, b, dims=((1,), (0,)), precision=None):
    return lax.dot_general(a, b, (dims, ((), ())), precision=precision, preferred_element_type=F32)


def kernel(
    n_sp,
    n_tp,
    n_dp,
    heads,
    condition,
    source,
    gain,
    conv_x,
    conv_b,
    conv_c,
    rate,
    out_gain,
    latent,
    context,
    mod_weight,
    w_x,
    w_b,
    w_c,
    w_dt,
    w_z,
    w_out,
    out,
    lat_all,
    ctx_buf,
    mod_buf,
    wx,
    wb,
    wc,
    wd,
    wz,
    wo,
    acts,
    edges,
    part,
    part_all,
    mods,
    halo,
    hid,
    snd_a,
    rcv_a,
    tot,
    snd_b,
    rcv_b,
    snd_o,
    rcv_o,
    local_sem,
    dp_send,
    dp_recv,
    lat_send,
    lat_recv,
    mod1_send,
    mod1_recv,
    mod2_send,
    mod2_recv,
    edge_send,
    edge_recv,
    a_send,
    a_recv,
    t_send,
    t_recv,
    b_send,
    b_recv,
    o_send,
    o_recv,
):
    s = lax.axis_index("sp")
    t = lax.axis_index("tp")
    d = lax.axis_index("dp")
    own_rows, width = latent.shape
    ctx_rows = context.shape[0]
    depth = mod_weight.shape[1]
    rows = n_tp * own_rows
    inner = w_x.shape[1]
    both = 2 * inner
    head_dim = inner // heads
    nh2 = 2 * heads

    def remote(src, dst, send, recv, **to):
        return pltpu.make_async_remote_copy(
            src_ref=src, dst_ref=dst, send_sem=send, recv_sem=recv, device_id=to, device_id_type=MESH
        )

    local = []

    def fetch(src, dst):
        copy = pltpu.make_async_copy(src, dst, local_sem.at[len(local)])
        copy.start()
        local.append(copy)
        return copy

    mod_copy = fetch(mod_weight, mod_buf)
    lat_copy = fetch(latent, lat_all.at[t])
    ctx_copy = fetch(context, ctx_buf)
    lat_moves = []
    for k in range(1, n_tp):
        lat_moves.append(
            remote(latent, lat_all.at[t], lat_send.at[k], lat_recv.at[k], tp=lax.rem(t + k, n_tp))
        )
        lat_moves[-1].start()
    weight_moves = []
    pairs = ((w_x, wx), (w_b, wb), (w_dt, wd), (w_c, wc), (w_z, wz), (w_out, wo))
    for i, (src, dst) in enumerate(pairs):
        count = src.shape[0]
        place = dst.at[d] if src is w_dt else dst.at[pl.ds(d * count, count)]
        for k in range(1, n_dp):
            at = i * n_dp + k
            weight_moves.append(
                remote(src, place, dp_send.at[at], dp_recv.at[at], dp=lax.rem(d + k, n_dp))
            )
            weight_moves[-1].start()
        fetch(src, place)

    active = silu(jnp.concatenate([condition[...].astype(F32), row_of(source)], axis=0))
    for j in range(n_sp):
        acts[j, 0:2] = active[:, j * depth : (j + 1) * depth]
    own_acts = jnp.concatenate([acts[s, 0:2], jnp.zeros((PAD - 2, depth), F32)], axis=0).astype(BF16)
    mod_copy.wait()
    pieces = [dot(own_acts, mod_buf[k])[0:2] for k in range(mod_buf.shape[0])]
    cols = pieces[0].shape[1]
    part[...] = jnp.concatenate(pieces + [jnp.zeros((2, cols), F32)], axis=0)
    moves = []
    for k in range(1, n_sp):
        moves.append(
            remote(part, part_all.at[k], mod1_send.at[k], mod1_recv.at[k], sp=lax.rem(s + k, n_sp))
        )
        moves[-1].start()
    lat_copy.wait()
    edges[0] = lat_all[t, 0:1].astype(F32)
    edges[1] = lat_all[t, own_rows - 1 : own_rows].astype(F32)
    ctx_copy.wait()
    edges[2] = ctx_buf[0:1].astype(F32)
    edges[3] = ctx_buf[ctx_rows - 1 : ctx_rows].astype(F32)
    up, down = lax.rem(s + 1, n_sp), lax.rem(s + n_sp - 1, n_sp)
    ctx_up = remote(edges.at[3], halo.at[2], edge_send.at[0], edge_recv.at[2], sp=up)
    ctx_down = remote(edges.at[2], halo.at[3], edge_send.at[1], edge_recv.at[3], sp=down)
    ctx_up.start()
    ctx_down.start()
    lat_up = [
        remote(edges.at[1], halo.at[0], edge_send.at[2 + u], edge_recv.at[0], sp=up, tp=u)
        for u in range(n_tp)
    ]
    lat_down = [
        remote(edges.at[0], halo.at[1], edge_send.at[2 + n_tp + u], edge_recv.at[1], sp=down, tp=u)
        for u in range(n_tp)
    ]

    @pl.when(t == n_tp - 1)
    def _():
        for copy in lat_up:
            copy.start()

    @pl.when(t == 0)
    def _():
        for copy in lat_down:
            copy.start()

    summed = part[...]
    for k in range(1, n_sp):
        moves[k - 1].wait()
        summed = summed + part_all[k]
    mods[t] = summed
    moves = []
    for k in range(1, n_tp):
        moves.append(
            remote(mods.at[t], mods.at[t], mod2_send.at[k], mod2_recv.at[k], tp=lax.rem(t + k, n_tp))
        )
        moves[-1].start()
    for copy in moves:
        copy.wait()

    def vector(row):
        return jnp.concatenate([mods[c][row : row + 1] for c in range(n_tp)], axis=1)

    def normed(v, gains, shift):
        return v * lax.rsqrt(jnp.mean(v * v, axis=1, keepdims=True) + EPSILON) * gains + shift

    gain_row = row_of(gain)
    lat_shift, ctx_shift = vector(0), vector(1)
    lat_gain = gain_row * (1.0 + vector(2))
    ctx_gain = gain_row * (1.0 + vector(3))
    step_rows = min(32, ctx_rows)
    for r in range(0, ctx_rows, step_rows):
        block = ctx_buf[r : r + step_rows].astype(F32)
        hid[rows + PAD + r : rows + PAD + r + step_rows] = normed(block, ctx_gain, ctx_shift).astype(BF16)
    for copy in lat_moves:
        copy.wait()
    for u in range(n_tp):
        hid[u * own_rows : (u + 1) * own_rows] = normed(
            lat_all[u].astype(F32), lat_gain, lat_shift
        ).astype(BF16)
    ctx_up.wait_send()
    ctx_down.wait_send()
    ctx_up.wait_recv()
    ctx_down.wait_recv()
    lat_up[0].wait_recv()
    lat_down[0].wait_recv()

    @pl.when(t == n_tp - 1)
    def _():
        for copy in lat_up:
            copy.wait_send()

    @pl.when(t == 0)
    def _():
        for copy in lat_down:
            copy.wait_send()

    hid[rows : rows + PAD] = jnp.concatenate(
        [
            normed(halo[0], lat_gain, lat_shift),
            normed(halo[1], lat_gain, lat_shift),
            normed(halo[2], ctx_gain, ctx_shift),
            normed(halo[3], ctx_gain, ctx_shift),
            jnp.zeros((PAD - 4, width), F32),
        ],
        axis=0,
    ).astype(BF16)
    for copy in weight_moves:
        copy.wait()
    for copy in local[3:]:
        copy.wait()

    has_before = s > 0
    has_after = s < n_sp - 1

    def shaped(values, before, after, taps):
        count = values.shape[0]
        at = lax.broadcasted_iota(jnp.int32, values.shape, 0)
        before = jnp.where(has_before, before, 0.0)
        after = jnp.where(has_after, after, 0.0)
        earlier = jnp.where(at == 0, before, pltpu.roll(values, 1, 0))
        later = jnp.where(at == count - 1, after, pltpu.roll(values, count - 1, 0))
        w = taps[...].astype(F32)
        return silu(earlier * w[0:1] + values * w[1:2] + later * w[2:3]).astype(BF16)

    def project(weight, count):
        return dot(hid[0:count], weight[...]).astype(BF16).astype(F32)

    total = rows + PAD + ctx_rows
    px = project(wx, total)
    x_in = shaped(px[0:rows], px[rows : rows + 1], px[rows + 1 : rows + 2], conv_x).astype(F32)
    cx_in = shaped(
        px[rows + PAD :], px[rows + 2 : rows + 3], px[rows + 3 : rows + 4], conv_x
    ).astype(F32)
    pb = project(wb, total)
    b_in = shaped(pb[0:rows], pb[rows : rows + 1], pb[rows + 1 : rows + 2], conv_b)
    cb_in = shaped(pb[rows + PAD :], pb[rows + 2 : rows + 3], pb[rows + 3 : rows + 4], conv_b)
    features = None
    half = wd.shape[3]
    for r in range(n_dp):
        taps = jnp.concatenate(
            [wd[r, 0].astype(F32), wd[r, 1].astype(F32), jnp.zeros((LANES - nh2, half), F32)], axis=0
        ).astype(BF16)
        one = dot(hid[0:total, r * half : (r + 1) * half], taps, ((1,), (1,)))
        features = one if features is None else features + one
    step_all = softplus(features.astype(BF16).astype(F32))
    rates = jnp.concatenate([rate[0:1], rate[1:2], jnp.zeros((1, LANES - nh2), F32)], axis=1)

    spread_at = lax.broadcasted_iota(jnp.int32, (LANES, both), 0)
    spread_to = lax.broadcasted_iota(jnp.int32, (LANES, both), 1) // head_dim
    spreader = jnp.where((spread_to == spread_at) | (spread_to + nh2 == spread_at), 1.0, 0.0).astype(BF16)

    def expand(v):
        lane = lax.broadcasted_iota(jnp.int32, v.shape, 1)
        high = v.astype(BF16).astype(F32)
        low = pltpu.roll(v - high, nh2, 1)
        packed = jnp.where(lane < nh2, high, jnp.where(lane < 2 * nh2, low, 0.0))
        return dot(packed.astype(BF16), spreader)

    def running(steps):
        count = steps.shape[0]
        logs = -rates * steps
        a = lax.broadcasted_iota(jnp.int32, (count, count), 0)
        b = lax.broadcasted_iota(jnp.int32, (count, count), 1)
        lower = jnp.where(a >= b, 1.0, 0.0)
        upper = jnp.where(a <= b, 1.0, 0.0)
        lane = lax.broadcasted_iota(jnp.int32, logs.shape, 1)
        sums = jnp.where(
            lane < heads,
            dot(lower, logs, precision=lax.Precision.HIGHEST),
            dot(upper, logs, precision=lax.Precision.HIGHEST),
        )
        row_lane = lax.broadcasted_iota(jnp.int32, (1, LANES), 1)
        ends = jnp.where(row_lane < heads, sums[count - 1 : count], sums[0:1])
        return sums, ends

    def moved(values, steps):
        wide = jnp.concatenate([values, values], axis=1)
        return (wide * expand(steps)).astype(BF16)

    c_steps = step_all[rows + PAD :]
    c_sums, c_ends = running(c_steps)
    c_moved = moved(cx_in, c_steps)
    c_scaled = (c_moved.astype(F32) * expand(jnp.exp(c_ends - c_sums))).astype(BF16)
    c_state = dot(cb_in, c_scaled, ((0,), (0,)))
    l_steps = step_all[0:rows]
    l_sums, l_ends = running(l_steps)
    l_moved = moved(x_in, l_steps)
    l_scaled = (l_moved.astype(F32) * expand(jnp.exp(l_ends - l_sums))).astype(BF16)
    l_state = dot(b_in, l_scaled, ((0,), (0,)))
    state_rows = STATE // n_sp
    for r in range(n_sp):
        cut = slice(r * state_rows, (r + 1) * state_rows)
        snd_a[r, :, 0:both] = c_state[cut].astype(BF16)
        snd_a[r, :, both : 2 * both] = l_state[cut].astype(BF16)
    ends = jnp.exp(jnp.concatenate([c_ends, l_ends, jnp.zeros((6, LANES), F32)], axis=0))
    tot[s] = expand(ends)
    a_moves, t_moves = [], []
    for k in range(1, n_sp):
        to = lax.rem(s + k, n_sp)
        a_moves.append(remote(snd_a.at[to], rcv_a.at[s], a_send.at[k], a_recv.at[k], sp=to))
        a_moves[-1].start()
        t_moves.append(remote(tot.at[s], tot.at[s], t_send.at[k], t_recv.at[k], sp=to))
        t_moves[-1].start()
    rcv_a[s] = snd_a[s]

    pc = project(wc, rows + PAD)
    c_in = shaped(pc[0:rows], pc[rows : rows + 1], pc[rows + 1 : rows + 2], conv_c)
    scores = dot(c_in, b_in, ((1,), (1,)))
    at_t = lax.broadcasted_iota(jnp.int32, (rows, rows), 0)
    at_s = lax.broadcasted_iota(jnp.int32, (rows, rows), 1)
    sums_t = jnp.transpose(l_sums)

    def weights(lane, keep):
        gap = l_sums[:, lane : lane + 1] - sums_t[lane : lane + 1]
        return jnp.where(keep, scores * jnp.exp(jnp.minimum(gap, 0.0)), 0.0).astype(BF16)

    pair = LANES // head_dim
    inside = []
    lane_head = lax.broadcasted_iota(jnp.int32, (rows, LANES), 1) // head_dim
    for p in range(heads // pair):
        cut = slice(p * LANES, (p + 1) * LANES)
        cut_b = slice(inner + p * LANES, inner + (p + 1) * LANES)
        source = jnp.concatenate([l_moved[:, cut], l_moved[:, cut_b]], axis=0)
        value = None
        for i in range(pair):
            h = p * pair + i
            w = jnp.concatenate([weights(h, at_t >= at_s), weights(heads + h, at_t <= at_s)], axis=1)
            one = dot(w, source)
            value = one if value is None else jnp.where(lane_head == i, one, value)
        inside.append(value)
    inside = jnp.concatenate(inside, axis=1)
    growth = expand(jnp.exp(l_sums))
    gate = silu(project(wz, rows))

    for copy in a_moves + t_moves:
        copy.wait()
    entering = None
    ctx_f = ctx_b = None
    for j in range(n_sp):
        mine = rcv_a[j, :, 0:inner].astype(F32)
        ctx_f = mine if ctx_f is None else ctx_f * tot[j, 0:1, 0:inner] + mine
        i = n_sp - 1 - j
        mine = rcv_a[i, :, inner:both].astype(F32)
        ctx_b = mine if ctx_b is None else ctx_b * tot[i, 0:1, inner:both] + mine
    for j in range(n_sp):
        snd_b[j, :, 0:inner] = ctx_f.astype(BF16)
        ctx_f = ctx_f * tot[j, 1:2, 0:inner] + rcv_a[j, :, both : both + inner].astype(F32)
        i = n_sp - 1 - j
        snd_b[i, :, inner:both] = ctx_b.astype(BF16)
        ctx_b = ctx_b * tot[i, 1:2, inner:both] + rcv_a[i, :, both + inner : 2 * both].astype(F32)
    b_moves = []
    for k in range(1, n_sp):
        to = lax.rem(s + k, n_sp)
        b_moves.append(remote(snd_b.at[to], rcv_b.at[s], b_send.at[k], b_recv.at[k], sp=to))
        b_moves[-1].start()
    rcv_b[s] = snd_b[s]
    for copy in b_moves:
        copy.wait()
    entering = jnp.concatenate([rcv_b[r] for r in range(n_sp)], axis=0)
    carried = dot(c_in, entering) * growth
    gated = (inside + carried[:, 0:inner] + carried[:, inner:both]) * gate
    ny = (
        gated
        * lax.rsqrt(jnp.mean(gated * gated, axis=1, keepdims=True) + EPSILON)
        * row_of(out_gain)
    ).astype(BF16)

    chunks = n_tp
    chunk = width // chunks
    o_moves = []
    for c in range(chunks):
        cut = slice(c * chunk, (c + 1) * chunk)
        result = dot(ny, wo[:, cut]).astype(BF16)
        for u in range(n_tp):
            snd_o[c, u] = result[u * own_rows : (u + 1) * own_rows]
        for k in range(1, n_tp):
            to = lax.rem(t + k, n_tp)
            at = c * n_tp + k
            o_moves.append(remote(snd_o.at[c, to], rcv_o.at[c, k], o_send.at[at], o_recv.at[at], tp=to))
            o_moves[-1].start()
    for c in range(chunks):
        mixed = snd_o[c, t].astype(F32)
        for k in range(1, n_tp):
            o_moves[c * (n_tp - 1) + k - 1].wait()
            mixed = mixed + rcv_o[c, k].astype(F32)
        out[:, c * chunk : (c + 1) * chunk] = (mods[c][4:5] * mixed).astype(BF16)


def shards(
    latent,
    condition,
    context,
    context_source,
    mod_weight,
    norm_gain,
    w_x,
    w_b,
    w_c,
    w_z,
    w_dt,
    conv_x,
    conv_b,
    conv_c,
    decay_rate,
    out_gain,
    w_out,
):
    n_sp, n_tp, n_dp = lax.axis_size("sp"), lax.axis_size("tp"), lax.axis_size("dp")
    own_rows, width = latent.shape[1:]
    ctx_rows = context.shape[1]
    depth = mod_weight.shape[1]
    cols = mod_weight.shape[2]
    inner = w_x.shape[1]
    heads = decay_rate.shape[1]
    both = 2 * inner
    rows = n_tp * own_rows
    state_rows = STATE // n_sp
    chunk = width // n_tp
    vmem = pl.BlockSpec(memory_space=pltpu.VMEM)
    anywhere = pl.BlockSpec(memory_space=pl.ANY)
    dma = pltpu.SemaphoreType.DMA
    scratch = [
        pltpu.VMEM((n_tp, own_rows, width), BF16),
        pltpu.VMEM((ctx_rows, width), BF16),
        pltpu.VMEM(mod_weight.shape, BF16),
        pltpu.VMEM((w_x.shape[0] * n_dp, inner), BF16),
        pltpu.VMEM((w_b.shape[0] * n_dp, w_b.shape[1]), BF16),
        pltpu.VMEM((w_c.shape[0] * n_dp, w_c.shape[1]), BF16),
        pltpu.VMEM((n_dp, 2, heads, w_dt.shape[1]), BF16),
        pltpu.VMEM((w_z.shape[0] * n_dp, inner), BF16),
        pltpu.VMEM((w_out.shape[0] * n_dp, width), BF16),
        pltpu.VMEM((n_sp, 8, depth), F32),
        pltpu.VMEM((4, 1, width), F32),
        pltpu.VMEM((8, cols), F32),
        pltpu.VMEM((n_sp, 8, cols), F32),
        pltpu.VMEM((n_tp, 8, cols), F32),
        pltpu.VMEM((4, 1, width), F32),
        pltpu.VMEM((rows + PAD + ctx_rows, width), BF16),
        pltpu.VMEM((n_sp, state_rows, 2 * both), BF16),
        pltpu.VMEM((n_sp, state_rows, 2 * both), BF16),
        pltpu.VMEM((n_sp, 8, both), F32),
        pltpu.VMEM((n_sp, state_rows, both), BF16),
        pltpu.VMEM((n_sp, state_rows, both), BF16),
        pltpu.VMEM((n_tp, n_tp, own_rows, chunk), BF16),
        pltpu.VMEM((n_tp, n_tp, own_rows, chunk), BF16),
        dma((9,)),
        dma((6 * n_dp,)),
        dma((6 * n_dp,)),
        dma((n_tp,)),
        dma((n_tp,)),
        dma((n_sp,)),
        dma((n_sp,)),
        dma((n_tp,)),
        dma((n_tp,)),
        dma((2 + 2 * n_tp,)),
        dma((4,)),
        dma((n_sp,)),
        dma((n_sp,)),
        dma((n_sp,)),
        dma((n_sp,)),
        dma((n_sp,)),
        dma((n_sp,)),
        dma((n_tp * n_tp,)),
        dma((n_tp * n_tp,)),
    ]
    result = pl.pallas_call(
        functools.partial(kernel, n_sp, n_tp, n_dp, heads),
        out_shape=jax.ShapeDtypeStruct((own_rows, width), BF16),
        in_specs=[vmem] * 8 + [anywhere] * 9,
        out_specs=vmem,
        scratch_shapes=scratch,
        compiler_params=pltpu.CompilerParams(
            has_side_effects=True, vmem_limit_bytes=62_000_000
        ),
    )(
        condition,
        context_source,
        norm_gain,
        conv_x,
        conv_b,
        conv_c,
        decay_rate,
        out_gain,
        latent[0],
        context[0],
        mod_weight,
        w_x,
        w_b,
        w_c,
        jnp.swapaxes(w_dt, 1, 2),
        w_z,
        w_out,
    )
    return result[None]


def solution(mesh):
    placed = (
        P("dp", ("sp", "tp"), None),
        P("dp", None),
        P("dp", "sp", None),
        P(),
        P(None, "sp", "tp"),
        P(),
        P("dp", "tp"),
        P("dp", "tp"),
        P("dp", "tp"),
        P("dp", "tp"),
        P(None, "dp", "tp"),
        P(None, "tp"),
        P(None, "tp"),
        P(None, "tp"),
        P(None, "tp"),
        P("tp"),
        P(("tp", "dp"), None),
    )
    return jax.shard_map(
        shards, mesh=mesh, in_specs=placed, out_specs=P("dp", ("sp", "tp"), None), check_vma=False
    )
```

profile of v0, /device:TPU:4, one launch (start us, length us, event | category | flops | bytes accessed | tf_op | source)
XLA Modules:
  0.0 204.9 jit_solution(16826409883446340801)
XLA Ops:
  0.0 203.4 %shard_map.163 = bf16[32,2048]{1,0:T(8,128)(2,1)} custom-call(bf16[1,2048]{1,0:T(2,128)(2,1)} %condition.1, bf16[2048]{0:T(1024)(128)(2,1)} %source.1, bf16[2048]{0:T(1024)(128)(2,1)} %gain.1, bf16[3,512]{1,0:T(4,128)(2,1)} %conv_x.1, bf16[3,128]{1,0:T(4,128)(2,1)} %conv_b.1, bf16[3,128]{1,0:T(4,128)(2,1)} %conv_c.1, f32[2,8]{1,0:T(2,128)} %rate.1, ...), custom_call_target="tpu_custom_call" | custom-call | tf_op jit(solution)/shard_map/pallas_call | solution.py:512
  203.4 1.6 copy.19
where the time goes:
time: 205 us
  Pallas kernels  203 us (99%)
    pallas_call x1, Pallas kernels, shards(): pl.pallas_call(functools.partial(kernel, n_sp, n_tp, n_dp, heads), out_sh...  203 us

commit v1 on v0

v1 whole, which is shorter than its diff:
```python
import functools

import jax
import jax.numpy as jnp
from jax import lax
from jax.experimental import pallas as pl
from jax.experimental.pallas import tpu as pltpu
from jax.sharding import PartitionSpec as P

STATE = 128
LANES = 128
PAD = 16
SIDE = 8
TILE = 16
EPSILON = 1e-06
MESH = pl.DeviceIdType.MESH
F32 = jnp.float32
BF16 = jnp.bfloat16


def silu(v):
    return v / (1.0 + jnp.exp(-v))


def softplus(v):
    return jnp.maximum(v, 0.0) + jnp.log1p(jnp.exp(-jnp.abs(v)))


def row_of(ref):
    return ref[...].astype(F32).reshape(1, ref.shape[0])


def dot(a, b, dims=((1,), (0,)), precision=None):
    return lax.dot_general(a, b, (dims, ((), ())), precision=precision, preferred_element_type=F32)


def far_first():
    def reach(k):
        return min(k, SIDE - k)

    steps = [(a, b) for a in range(SIDE) for b in range(SIDE) if a or b]
    return sorted(steps, key=lambda ab: -(reach(ab[0]) + reach(ab[1])))


def kernel(
    n_sp,
    n_tp,
    n_dp,
    heads,
    condition_in,
    source_in,
    gain_in,
    conv_x_in,
    conv_b_in,
    conv_c_in,
    rate_in,
    out_gain_in,
    latent,
    context,
    mod_weight,
    w_x,
    w_b,
    w_c,
    w_dt,
    w_z,
    w_out,
    out,
    condition,
    source,
    gain,
    conv_x,
    conv_b,
    conv_c,
    rate,
    out_gain,
    lat_all,
    ctx_buf,
    mod_buf,
    wx,
    wb,
    wc,
    wd,
    wz,
    wo,
    acts,
    edges,
    part,
    part_z,
    part_up,
    part_y,
    mods,
    halo,
    pre,
    hid,
    snd_c,
    rcv_c,
    snd_l,
    rcv_l,
    snd_t,
    rcv_t,
    snd_b,
    rcv_b,
    snd_o,
    rcv_o,
    local_sem,
    dp_send,
    dp_recv,
    lat_send,
    lat_recv,
    line_send,
    line_recv,
    mod_send,
    mod_recv,
    edge_send,
    edge_recv,
    flat_send,
    flat_recv,
    o_send,
    o_recv,
):
    s = lax.axis_index("sp")
    t = lax.axis_index("tp")
    d = lax.axis_index("dp")
    z = s // SIDE
    y = lax.rem(s, SIDE)
    own_rows, width = latent.shape
    ctx_rows = context.shape[0]
    depth = mod_weight.shape[1]
    rows = n_tp * own_rows
    inner = w_x.shape[1]
    both = 2 * inner
    head_dim = inner // heads
    nh2 = 2 * heads
    up, down = lax.rem(s + 1, n_sp), lax.rem(s + n_sp - 1, n_sp)

    def remote(src, dst, send, recv, **to):
        return pltpu.make_async_remote_copy(
            src_ref=src, dst_ref=dst, send_sem=send, recv_sem=recv, device_id=to, device_id_type=MESH
        )

    barrier = pltpu.get_barrier_semaphore()

    def greet(**to):
        pl.semaphore_signal(barrier, inc=1, device_id=to, device_id_type=MESH)

    def on_z(k):
        return lax.rem(z + k, SIDE) * SIDE + y

    def on_y(k):
        return z * SIDE + lax.rem(y + k, SIDE)

    for k in range(1, SIDE):
        greet(sp=on_z(k))
        greet(sp=on_y(k))
    for k in range(1, n_tp):
        greet(tp=lax.rem(t + k, n_tp))
    for k in range(1, n_dp):
        greet(dp=lax.rem(d + k, n_dp))
    greet(sp=up)
    greet(sp=down)
    greet(sp=down, tp=n_tp - 1)
    greet(sp=up, tp=0)

    local = []

    def fetch(src, dst):
        copy = pltpu.make_async_copy(src, dst, local_sem.at[len(local)])
        copy.start()
        local.append(copy)
        return copy

    early = [fetch(condition_in, condition), fetch(source_in, source), fetch(mod_weight, mod_buf)]
    lat_copy = fetch(latent, lat_all.at[t])
    ctx_copy = fetch(context, ctx_buf)
    small = [
        fetch(a, b)
        for a, b in (
            (gain_in, gain),
            (conv_x_in, conv_x),
            (conv_b_in, conv_b),
            (conv_c_in, conv_c),
            (rate_in, rate),
            (out_gain_in, out_gain),
        )
    ]
    pairs = ((w_x, wx), (w_b, wb), (w_dt, wd), (w_c, wc), (w_z, wz), (w_out, wo))
    places = []
    weight_copies = []
    for src, dst in pairs:
        count = src.shape[0]
        places.append(dst.at[d] if src is w_dt else dst.at[pl.ds(d * count, count)])
        weight_copies.append(fetch(src, places[-1]))

    for copy in early:
        copy.wait()
    acts[0:1] = condition[...].astype(F32)
    acts[1:2] = row_of(source)
    per = LANES // depth
    block = acts[0:2, pl.ds(pl.multiple_of((s // per) * LANES, LANES), LANES)]
    active = jnp.concatenate([silu(block), jnp.zeros((PAD - 2, LANES), F32)], axis=0)
    own_acts = active[:, 0:depth]
    for j in range(1, per):
        own_acts = jnp.where(lax.rem(s, per) == j, active[:, j * depth : (j + 1) * depth], own_acts)
    own_acts = own_acts.astype(BF16)
    pieces = [dot(own_acts, mod_buf[k])[0:2] for k in range(mod_buf.shape[0])]
    cols = pieces[0].shape[1]
    partial = jnp.concatenate(pieces + [jnp.zeros((2, cols), F32)], axis=0)
    part[...] = partial

    lat_copy.wait()
    edges[0] = lat_all[t, 0:1].astype(F32)
    edges[1] = lat_all[t, own_rows - 1 : own_rows].astype(F32)
    ctx_copy.wait()
    edges[2] = ctx_buf[0:1].astype(F32)
    edges[3] = ctx_buf[ctx_rows - 1 : ctx_rows].astype(F32)

    expected = 2 * (SIDE - 1) + n_tp - 1 + n_dp - 1 + 2
    expected = expected + jnp.where(t == n_tp - 1, n_tp, 0) + jnp.where(t == 0, n_tp, 0)
    pl.semaphore_wait(barrier, expected)

    def line(src, dst, place, phase):
        for k in range(1, SIDE):
            remote(src, dst.at[k - 1], line_send.at[phase], line_recv.at[phase], sp=place(k)).start()

    def line_wait(dst, phase):
        pltpu.make_async_copy(dst, dst, line_recv.at[phase]).wait()

    line(part, part_z, on_z, 0)
    lat_moves = []
    for k in range(1, n_tp):
        lat_moves.append(
            remote(latent, lat_all.at[t], lat_send.at[k], lat_recv.at[k], tp=lax.rem(t + k, n_tp))
        )
        lat_moves[-1].start()
    ctx_up = remote(edges.at[3], halo.at[2], edge_send.at[0], edge_recv.at[2], sp=up)
    ctx_down = remote(edges.at[2], halo.at[3], edge_send.at[1], edge_recv.at[3], sp=down)
    ctx_up.start()
    ctx_down.start()
    lat_up = [
        remote(edges.at[1], halo.at[0], edge_send.at[2 + u], edge_recv.at[0], sp=up, tp=u)
        for u in range(n_tp)
    ]
    lat_down = [
        remote(edges.at[0], halo.at[1], edge_send.at[2 + n_tp + u], edge_recv.at[1], sp=down, tp=u)
        for u in range(n_tp)
    ]

    @pl.when(t == n_tp - 1)
    def _():
        for copy in lat_up:
            copy.start()

    @pl.when(t == 0)
    def _():
        for copy in lat_down:
            copy.start()

    weight_moves = []
    for i, (src, dst) in enumerate(pairs):
        for k in range(1, n_dp):
            at = i * n_dp + k
            weight_moves.append(
                remote(src, places[i], dp_send.at[at], dp_recv.at[at], dp=lax.rem(d + k, n_dp))
            )
            weight_moves[-1].start()

    def normed(v):
        return v * lax.rsqrt(jnp.mean(v * v, axis=1, keepdims=True) + EPSILON)

    pre[rows + PAD : rows + PAD + ctx_rows] = normed(ctx_buf[...].astype(F32))

    line_wait(part_z, 0)
    summed = part[...]
    for k in range(1, SIDE):
        summed = summed + part_z[k - 1]
    part_up[...] = summed
    line(part_up, part_y, on_y, 1)

    for copy in lat_moves:
        copy.wait()
    for u in range(n_tp):
        pre[u * own_rows : (u + 1) * own_rows] = normed(lat_all[u].astype(F32))
    ctx_up.wait_recv()
    ctx_down.wait_recv()
    lat_up[0].wait_recv()
    lat_down[0].wait_recv()
    pre[rows : rows + PAD] = normed(
        jnp.concatenate([halo[0], halo[1], halo[2], halo[3], jnp.zeros((PAD - 4, width), F32)], axis=0)
    )

    line_wait(part_y, 1)
    summed = part_up[...]
    for k in range(1, SIDE):
        summed = summed + part_y[k - 1]
    mods[t] = summed
    moves = []
    for k in range(1, n_tp):
        moves.append(
            remote(mods.at[t], mods.at[t], mod_send.at[k], mod_recv.at[k], tp=lax.rem(t + k, n_tp))
        )
        moves[-1].start()
    for copy in small:
        copy.wait()
    for copy in moves:
        copy.wait()

    def vector(row):
        return jnp.concatenate([mods[c][row : row + 1] for c in range(n_tp)], axis=1)

    gain_row = row_of(gain)
    lat_shift, ctx_shift = vector(0), vector(1)
    lat_gain = gain_row * (1.0 + vector(2))
    ctx_gain = gain_row * (1.0 + vector(3))
    for u in range(n_tp):
        cut = slice(u * own_rows, (u + 1) * own_rows)
        hid[cut] = (pre[cut] * lat_gain + lat_shift).astype(BF16)
    at_row = lax.broadcasted_iota(jnp.int32, (PAD, width), 0)
    edge = pre[rows : rows + PAD]
    hid[rows : rows + PAD] = jnp.where(
        at_row < 2, edge * lat_gain + lat_shift, edge * ctx_gain + ctx_shift
    ).astype(BF16)
    hid[rows + PAD : rows + PAD + ctx_rows] = (
        pre[rows + PAD : rows + PAD + ctx_rows] * ctx_gain + ctx_shift
    ).astype(BF16)
    for copy in weight_moves:
        copy.wait()
    for copy in weight_copies:
        copy.wait()

    has_before = s > 0
    has_after = s < n_sp - 1

    def shaped(values, before, after, taps):
        count = values.shape[0]
        at = lax.broadcasted_iota(jnp.int32, values.shape, 0)
        before = jnp.where(has_before, before, 0.0)
        after = jnp.where(has_after, after, 0.0)
        earlier = jnp.where(at == 0, before, pltpu.roll(values, 1, 0))
        later = jnp.where(at == count - 1, after, pltpu.roll(values, count - 1, 0))
        w = taps[...].astype(F32)
        return silu(earlier * w[0:1] + values * w[1:2] + later * w[2:3]).astype(BF16)

    def project(weight, count):
        return dot(hid[0:count], weight[...]).astype(BF16).astype(F32)

    total = rows + PAD + ctx_rows
    spread_at = lax.broadcasted_iota(jnp.int32, (LANES, both), 0)
    spread_to = lax.broadcasted_iota(jnp.int32, (LANES, both), 1) // head_dim
    spreader = jnp.where((spread_to == spread_at) | (spread_to + nh2 == spread_at), 1.0, 0.0).astype(BF16)

    def expand(v):
        lane = lax.broadcasted_iota(jnp.int32, v.shape, 1)
        high = v.astype(BF16).astype(F32)
        low = pltpu.roll(v - high, nh2, 1)
        packed = jnp.where(lane < nh2, high, jnp.where(lane < 2 * nh2, low, 0.0))
        return dot(packed.astype(BF16), spreader)

    def running(steps):
        count = steps.shape[0]
        logs = -rates * steps
        a = lax.broadcasted_iota(jnp.int32, (count, count), 0)
        b = lax.broadcasted_iota(jnp.int32, (count, count), 1)
        lower = jnp.where(a >= b, 1.0, 0.0)
        upper = jnp.where(a <= b, 1.0, 0.0)
        lane = lax.broadcasted_iota(jnp.int32, logs.shape, 1)
        sums = jnp.where(
            lane < heads,
            dot(lower, logs, precision=lax.Precision.HIGHEST),
            dot(upper, logs, precision=lax.Precision.HIGHEST),
        )
        row_lane = lax.broadcasted_iota(jnp.int32, (1, LANES), 1)
        ends = jnp.where(row_lane < heads, sums[count - 1 : count], sums[0:1])
        return sums, ends

    def moved(values, steps):
        wide = jnp.concatenate([values, values], axis=1)
        return (wide * expand(steps)).astype(BF16)

    def spread_out(src, dst, phase):
        for a, b in far_first():
            to = lax.rem(z + a, SIDE) * SIDE + lax.rem(y + b, SIDE)
            remote(src.at[to], dst.at[s], flat_send.at[phase], flat_recv.at[phase], sp=to).start()
        dst[s] = src[s]

    def all_in(dst, phase):
        most = dst.at[pl.ds(0, n_sp - 1)]
        pltpu.make_async_copy(most, most, flat_recv.at[phase]).wait()

    def tiles(dst, state):
        for a in range(SIDE):
            for b in range(SIDE):
                dst[a * SIDE + b] = state[
                    b * TILE : (b + 1) * TILE, a * LANES : (a + 1) * LANES
                ].astype(BF16)

    features = None
    half = wd.shape[3]
    for r in range(n_dp):
        taps = jnp.concatenate(
            [wd[r, 0].astype(F32), wd[r, 1].astype(F32), jnp.zeros((LANES - nh2, half), F32)], axis=0
        ).astype(BF16)
        one = dot(hid[0:total, r * half : (r + 1) * half], taps, ((1,), (1,)))
        features = one if features is None else features + one
    step_all = softplus(features.astype(BF16).astype(F32))
    rates = jnp.concatenate([rate[0:1], rate[1:2], jnp.zeros((1, LANES - nh2), F32)], axis=1)
    c_steps = step_all[rows + PAD :]
    c_sums, c_ends = running(c_steps)
    l_steps = step_all[0:rows]
    l_sums, l_ends = running(l_steps)
    ends = expand(jnp.exp(jnp.concatenate([c_ends, l_ends, jnp.zeros((6, LANES), F32)], axis=0)))
    for a in range(SIDE):
        lanes = ends[0:2, a * LANES : (a + 1) * LANES]
        for b in range(SIDE):
            snd_t[a * SIDE + b] = lanes
    spread_out(snd_t, rcv_t, 0)

    px = project(wx, total)
    cx_in = shaped(
        px[rows + PAD :], px[rows + 2 : rows + 3], px[rows + 3 : rows + 4], conv_x
    ).astype(F32)
    pb = project(wb, total)
    cb_in = shaped(pb[rows + PAD :], pb[rows + 2 : rows + 3], pb[rows + 3 : rows + 4], conv_b)
    c_moved = moved(cx_in, c_steps)
    c_scaled = (c_moved.astype(F32) * expand(jnp.exp(c_ends - c_sums))).astype(BF16)
    tiles(snd_c, dot(cb_in, c_scaled, ((0,), (0,))))
    spread_out(snd_c, rcv_c, 1)

    x_in = shaped(px[0:rows], px[rows : rows + 1], px[rows + 1 : rows + 2], conv_x).astype(F32)
    b_in = shaped(pb[0:rows], pb[rows : rows + 1], pb[rows + 1 : rows + 2], conv_b)
    l_moved = moved(x_in, l_steps)
    l_scaled = (l_moved.astype(F32) * expand(jnp.exp(l_ends - l_sums))).astype(BF16)
    tiles(snd_l, dot(b_in, l_scaled, ((0,), (0,))))
    spread_out(snd_l, rcv_l, 2)

    pc = project(wc, rows + PAD)
    c_in = shaped(pc[0:rows], pc[rows : rows + 1], pc[rows + 1 : rows + 2], conv_c)
    scores = dot(c_in, b_in, ((1,), (1,)))
    at_t = lax.broadcasted_iota(jnp.int32, (rows, rows), 0)
    at_s = lax.broadcasted_iota(jnp.int32, (rows, rows), 1)
    sums_t = jnp.transpose(l_sums)

    def weights(lane, keep):
        gap = l_sums[:, lane : lane + 1] - sums_t[lane : lane + 1]
        return jnp.where(keep, scores * jnp.exp(jnp.minimum(gap, 0.0)), 0.0).astype(BF16)

    pair = LANES // head_dim
    inside = []
    lane_head = lax.broadcasted_iota(jnp.int32, (rows, LANES), 1) // head_dim
    for p in range(heads // pair):
        cut = slice(p * LANES, (p + 1) * LANES)
        cut_b = slice(inner + p * LANES, inner + (p + 1) * LANES)
        sources = jnp.concatenate([l_moved[:, cut], l_moved[:, cut_b]], axis=0)
        value = None
        for i in range(pair):
            h = p * pair + i
            w = jnp.concatenate([weights(h, at_t >= at_s), weights(heads + h, at_t <= at_s)], axis=1)
            one = dot(w, sources)
            value = one if value is None else jnp.where(lane_head == i, one, value)
        inside.append(value)
    inside = jnp.concatenate(inside, axis=1)
    growth = expand(jnp.exp(l_sums))
    gate = silu(project(wz, rows))

    forward = z < SIDE // 2

    def place(j):
        return jnp.where(forward, j, n_sp - 1 - j)

    all_in(rcv_t, 0)
    all_in(rcv_c, 1)
    state = jnp.zeros((TILE, LANES), F32)

    def context_step(j, state):
        i = place(j)
        return state * rcv_t[i, 0:1] + rcv_c[i].astype(F32)

    state = lax.fori_loop(0, n_sp, context_step, state, unroll=8)
    all_in(rcv_l, 2)

    def latent_step(j, state):
        i = place(j)
        snd_b[i] = state.astype(BF16)
        return state * rcv_t[i, 1:2] + rcv_l[i].astype(F32)

    lax.fori_loop(0, n_sp, latent_step, state, unroll=8)
    spread_out(snd_b, rcv_b, 3)
    all_in(rcv_b, 3)
    entering = jnp.concatenate(
        [rcv_b[a * SIDE : (a + 1) * SIDE].reshape(STATE, LANES) for a in range(SIDE)], axis=1
    )
    carried = dot(c_in, entering) * growth
    gated = (inside + carried[:, 0:inner] + carried[:, inner:both]) * gate
    ny = (
        gated
        * lax.rsqrt(jnp.mean(gated * gated, axis=1, keepdims=True) + EPSILON)
        * row_of(out_gain)
    ).astype(BF16)

    chunks = n_tp
    chunk = width // chunks
    o_moves = []
    for c in range(chunks):
        cut = slice(c * chunk, (c + 1) * chunk)
        result = dot(ny, wo[:, cut]).astype(BF16)
        for u in range(n_tp):
            snd_o[c, u] = result[u * own_rows : (u + 1) * own_rows]
        for k in range(1, n_tp):
            to = lax.rem(t + k, n_tp)
            at = c * n_tp + k
            o_moves.append(remote(snd_o.at[c, to], rcv_o.at[c, k], o_send.at[at], o_recv.at[at], tp=to))
            o_moves[-1].start()

    for phase, sent in ((0, part_z), (1, part_y)):
        pltpu.make_async_copy(sent, sent, line_send.at[phase]).wait()
    for phase, sent in ((0, rcv_t), (1, rcv_c), (2, rcv_l), (3, rcv_b)):
        most = sent.at[pl.ds(0, n_sp - 1)]
        pltpu.make_async_copy(most, most, flat_send.at[phase]).wait()
    ctx_up.wait_send()
    ctx_down.wait_send()

    @pl.when(t == n_tp - 1)
    def _():
        for copy in lat_up:
            copy.wait_send()

    @pl.when(t == 0)
    def _():
        for copy in lat_down:
            copy.wait_send()

    for c in range(chunks):
        mixed = snd_o[c, t].astype(F32)
        for k in range(1, n_tp):
            o_moves[c * (n_tp - 1) + k - 1].wait()
            mixed = mixed + rcv_o[c, k].astype(F32)
        out[:, c * chunk : (c + 1) * chunk] = (mods[c][4:5] * mixed).astype(BF16)


def shards(
    latent,
    condition,
    context,
    context_source,
    mod_weight,
    norm_gain,
    w_x,
    w_b,
    w_c,
    w_z,
    w_dt,
    conv_x,
    conv_b,
    conv_c,
    decay_rate,
    out_gain,
    w_out,
):
    n_sp, n_tp, n_dp = lax.axis_size("sp"), lax.axis_size("tp"), lax.axis_size("dp")
    assert n_sp == SIDE * SIDE
    own_rows, width = latent.shape[1:]
    ctx_rows = context.shape[1]
    cols = mod_weight.shape[2]
    inner = w_x.shape[1]
    heads = decay_rate.shape[1]
    assert STATE == SIDE * TILE and 2 * inner == SIDE * LANES
    rows = n_tp * own_rows
    total = rows + PAD + ctx_rows
    chunk = width // n_tp
    vmem = pl.BlockSpec(memory_space=pltpu.VMEM)
    anywhere = pl.BlockSpec(memory_space=pl.ANY)
    dma = pltpu.SemaphoreType.DMA
    args = (
        condition,
        context_source,
        norm_gain,
        conv_x,
        conv_b,
        conv_c,
        decay_rate,
        out_gain,
        latent[0],
        context[0],
        mod_weight,
        w_x,
        w_b,
        w_c,
        jnp.swapaxes(w_dt, 1, 2),
        w_z,
        w_out,
    )
    tiles = pltpu.VMEM((n_sp, TILE, LANES), BF16)
    scratch = [pltpu.VMEM(a.shape, a.dtype) for a in args[:8]] + [
        pltpu.VMEM((n_tp, own_rows, width), BF16),
        pltpu.VMEM((ctx_rows, width), BF16),
        pltpu.VMEM(mod_weight.shape, BF16),
        pltpu.VMEM((w_x.shape[0] * n_dp, inner), BF16),
        pltpu.VMEM((w_b.shape[0] * n_dp, w_b.shape[1]), BF16),
        pltpu.VMEM((w_c.shape[0] * n_dp, w_c.shape[1]), BF16),
        pltpu.VMEM((n_dp, 2, heads, w_dt.shape[1]), BF16),
        pltpu.VMEM((w_z.shape[0] * n_dp, inner), BF16),
        pltpu.VMEM((w_out.shape[0] * n_dp, width), BF16),
        pltpu.VMEM((8, width), F32),
        pltpu.VMEM((4, 1, width), F32),
        pltpu.VMEM((8, cols), F32),
        pltpu.VMEM((SIDE - 1, 8, cols), F32),
        pltpu.VMEM((8, cols), F32),
        pltpu.VMEM((SIDE - 1, 8, cols), F32),
        pltpu.VMEM((n_tp, 8, cols), F32),
        pltpu.VMEM((4, 1, width), F32),
        pltpu.VMEM((total, width), F32),
        pltpu.VMEM((total, width), BF16),
        tiles,
        tiles,
        tiles,
        tiles,
        pltpu.VMEM((n_sp, 2, LANES), F32),
        pltpu.VMEM((n_sp, 2, LANES), F32),
        tiles,
        tiles,
        pltpu.VMEM((n_tp, n_tp, own_rows, chunk), BF16),
        pltpu.VMEM((n_tp, n_tp, own_rows, chunk), BF16),
        dma((17,)),
        dma((6 * n_dp,)),
        dma((6 * n_dp,)),
        dma((n_tp,)),
        dma((n_tp,)),
        dma((2,)),
        dma((2,)),
        dma((n_tp,)),
        dma((n_tp,)),
        dma((2 + 2 * n_tp,)),
        dma((4,)),
        dma((4,)),
        dma((4,)),
        dma((n_tp * n_tp,)),
        dma((n_tp * n_tp,)),
    ]
    result = pl.pallas_call(
        functools.partial(kernel, n_sp, n_tp, n_dp, heads),
        out_shape=jax.ShapeDtypeStruct((own_rows, width), BF16),
        in_specs=[anywhere] * len(args),
        out_specs=vmem,
        scratch_shapes=scratch,
        compiler_params=pltpu.CompilerParams(
            collective_id=0, has_side_effects=True, vmem_limit_bytes=62_000_000
        ),
    )(*args)
    return result[None]


def solution(mesh):
    placed = (
        P("dp", ("sp", "tp"), None),
        P("dp", None),
        P("dp", "sp", None),
        P(),
        P(None, "sp", "tp"),
        P(),
        P("dp", "tp"),
        P("dp", "tp"),
        P("dp", "tp"),
        P("dp", "tp"),
        P(None, "dp", "tp"),
        P(None, "tp"),
        P(None, "tp"),
        P(None, "tp"),
        P(None, "tp"),
        P("tp"),
        P(("tp", "dp"), None),
    )
    return jax.shard_map(
        shards, mesh=mesh, in_specs=placed, out_specs=P("dp", ("sp", "tp"), None), check_vma=False
    )
```

time: 205 us -> 62.1 us (0.30)
  the two profiles are of different devices: /device:TPU:4 before, /device:TPU:8 now
where the time goes in v1:
time: 62.1 us; the launch traced here: 61.9 us
  Pallas kernels  60.3 us (97%)
  local copies, waits for them, and re-layouts  1.57 us (3%)
    pallas_call x1, Pallas kernels, shards(): pl.pallas_call(functools.partial(kernel, n_sp, n_tp, n_dp, heads), out_sh...  60.3 us
    unnamed x1, local copies, waits for them, and re-layouts  1.57 us

profile of v1, /device:TPU:8, one launch (start us, length us, event | category | flops | bytes accessed | tf_op | source)
XLA Modules:
  0.0 61.9 jit_solution(2616089784058729657)
XLA Ops:
  0.0 60.3 %shard_map.163 = bf16[32,2048]{1,0:T(8,128)(2,1)} custom-call(bf16[1,2048]{1,0:T(2,128)(2,1)} %condition_in.1, bf16[2048]{0:T(1024)(128)(2,1)} %source_in.1, bf16[2048]{0:T(1024)(128)(2,1)} %gain_in.1, bf16[3,512]{1,0:T(4,128)(2,1)} %conv_x_in.1, bf16[3,128]{1,0:T(4,128)(2,1)} %conv_b_in.1, bf16[3,128]{1,0:T(4,128)(2,1)} %conv_c_in.1, f32[2,8]{1,0:T(2,128)} %rate_in.1, ...), custom_call_target="tpu_custom_call" | custom-call | tf_op jit(solution)/shard_map/pallas_call | solution.py:638
  60.3 1.6 %copy.19 = bf16[1,32,2048]{2,1,0:T(8,128)(2,1)} copy(bf16[1,32,2048]{2,1,0:T(8,128)(2,1)} %bitcast.4) | data formatting | bytes 262144

commit v2 on v1

--- a/solution.py
+++ b/solution.py
@@ -92,6 +92,7 @@
     halo,
     pre,
     hid,
+    c_full,
     snd_c,
     rcv_c,
     snd_l,
@@ -111,6 +112,8 @@
     line_recv,
     mod_send,
     mod_recv,
+    ctx_send,
+    ctx_recv,
     edge_send,
     edge_recv,
     flat_send,
@@ -124,7 +127,8 @@
     z = s // SIDE
     y = lax.rem(s, SIDE)
     own_rows, width = latent.shape
-    ctx_rows = context.shape[0]
+    own_ctx = context.shape[0]
+    ctx_rows = SIDE * own_ctx
     depth = mod_weight.shape[1]
     rows = n_tp * own_rows
     inner = w_x.shape[1]
@@ -156,8 +160,9 @@
         greet(tp=lax.rem(t + k, n_tp))
     for k in range(1, n_dp):
         greet(dp=lax.rem(d + k, n_dp))
-    greet(sp=up)
-    greet(sp=down)
+    z_up, z_down = lax.rem(z + 1, SIDE) * SIDE, lax.rem(z + SIDE - 1, SIDE) * SIDE
+    greet(sp=z_down + SIDE - 1)
+    greet(sp=z_up)
     greet(sp=down, tp=n_tp - 1)
     greet(sp=up, tp=0)
 
@@ -171,7 +176,7 @@
 
     early = [fetch(condition_in, condition), fetch(source_in, source), fetch(mod_weight, mod_buf)]
     lat_copy = fetch(latent, lat_all.at[t])
-    ctx_copy = fetch(context, ctx_buf)
+    ctx_copy = fetch(context, ctx_buf.at[y])
     small = [
         fetch(a, b)
         for a, b in (
@@ -205,16 +210,17 @@
     pieces = [dot(own_acts, mod_buf[k])[0:2] for k in range(mod_buf.shape[0])]
     cols = pieces[0].shape[1]
     partial = jnp.concatenate(pieces + [jnp.zeros((2, cols), F32)], axis=0)
-    part[...] = partial
+    part[...] = partial.astype(BF16)
 
     lat_copy.wait()
     edges[0] = lat_all[t, 0:1].astype(F32)
     edges[1] = lat_all[t, own_rows - 1 : own_rows].astype(F32)
     ctx_copy.wait()
-    edges[2] = ctx_buf[0:1].astype(F32)
-    edges[3] = ctx_buf[ctx_rows - 1 : ctx_rows].astype(F32)
-
-    expected = 2 * (SIDE - 1) + n_tp - 1 + n_dp - 1 + 2
+    edges[2] = ctx_buf[y, 0:1].astype(F32)
+    edges[3] = ctx_buf[y, own_ctx - 1 : own_ctx].astype(F32)
+
+    expected = 2 * (SIDE - 1) + n_tp - 1 + n_dp - 1
+    expected = expected + jnp.where(y == SIDE - 1, SIDE, 0) + jnp.where(y == 0, SIDE, 0)
     expected = expected + jnp.where(t == n_tp - 1, n_tp, 0) + jnp.where(t == 0, n_tp, 0)
     pl.semaphore_wait(barrier, expected)
 
@@ -232,18 +238,34 @@
             remote(latent, lat_all.at[t], lat_send.at[k], lat_recv.at[k], tp=lax.rem(t + k, n_tp))
         )
         lat_moves[-1].start()
-    ctx_up = remote(edges.at[3], halo.at[2], edge_send.at[0], edge_recv.at[2], sp=up)
-    ctx_down = remote(edges.at[2], halo.at[3], edge_send.at[1], edge_recv.at[3], sp=down)
-    ctx_up.start()
-    ctx_down.start()
+    for k in range(1, SIDE):
+        remote(context, ctx_buf.at[y], ctx_send.at[k], ctx_recv.at[k], sp=on_y(k)).start()
+    ctx_up = [
+        remote(edges.at[3], halo.at[2], edge_send.at[j], edge_recv.at[2], sp=z_up + j) for j in range(SIDE)
+    ]
+    ctx_down = [
+        remote(edges.at[2], halo.at[3], edge_send.at[SIDE + j], edge_recv.at[3], sp=z_down + j)
+        for j in range(SIDE)
+    ]
+    first = 2 * SIDE
     lat_up = [
-        remote(edges.at[1], halo.at[0], edge_send.at[2 + u], edge_recv.at[0], sp=up, tp=u)
+        remote(edges.at[1], halo.at[0], edge_send.at[first + u], edge_recv.at[0], sp=up, tp=u)
         for u in range(n_tp)
     ]
     lat_down = [
-        remote(edges.at[0], halo.at[1], edge_send.at[2 + n_tp + u], edge_recv.at[1], sp=down, tp=u)
+        remote(edges.at[0], halo.at[1], edge_send.at[first + n_tp + u], edge_recv.at[1], sp=down, tp=u)
         for u in range(n_tp)
     ]
+
+    @pl.when(y == SIDE - 1)
+    def _():
+        for copy in ctx_up:
+            copy.start()
+
+    @pl.when(y == 0)
+    def _():
+        for copy in ctx_down:
+            copy.start()
 
     @pl.when(t == n_tp - 1)
     def _():
@@ -267,21 +289,25 @@
     def normed(v):
         return v * lax.rsqrt(jnp.mean(v * v, axis=1, keepdims=True) + EPSILON)
 
-    pre[rows + PAD : rows + PAD + ctx_rows] = normed(ctx_buf[...].astype(F32))
-
     line_wait(part_z, 0)
-    summed = part[...]
+    summed = partial
     for k in range(1, SIDE):
-        summed = summed + part_z[k - 1]
-    part_up[...] = summed
+        summed = summed + part_z[k - 1].astype(F32)
+    part_up[...] = summed.astype(BF16)
     line(part_up, part_y, on_y, 1)
 
     for copy in lat_moves:
         copy.wait()
     for u in range(n_tp):
         pre[u * own_rows : (u + 1) * own_rows] = normed(lat_all[u].astype(F32))
-    ctx_up.wait_recv()
-    ctx_down.wait_recv()
+    for k in range(1, SIDE):
+        remote(context, ctx_buf.at[y], ctx_send.at[k], ctx_recv.at[k], sp=on_y(k)).wait()
+    for j in range(0, SIDE, 2):
+        pre[rows + PAD + j * own_ctx : rows + PAD + (j + 2) * own_ctx] = normed(
+            ctx_buf[j : j + 2].astype(F32).reshape(2 * own_ctx, width)
+        )
+    ctx_up[0].wait_recv()
+    ctx_down[0].wait_recv()
     lat_up[0].wait_recv()
     lat_down[0].wait_recv()
     pre[rows : rows + PAD] = normed(
@@ -289,9 +315,8 @@
     )
 
     line_wait(part_y, 1)
-    summed = part_up[...]
     for k in range(1, SIDE):
-        summed = summed + part_y[k - 1]
+        summed = summed + part_y[k - 1].astype(F32)
     mods[t] = summed
     moves = []
     for k in range(1, n_tp):
@@ -327,10 +352,7 @@
     for copy in weight_copies:
         copy.wait()
 
-    has_before = s > 0
-    has_after = s < n_sp - 1
-
-    def shaped(values, before, after, taps):
+    def shaped(values, before, after, taps, has_before=s > 0, has_after=s < n_sp - 1):
         count = values.shape[0]
         at = lax.broadcasted_iota(jnp.int32, values.shape, 0)
         before = jnp.where(has_before, before, 0.0)
@@ -409,28 +431,37 @@
     l_sums, l_ends = running(l_steps)
     ends = expand(jnp.exp(jnp.concatenate([c_ends, l_ends, jnp.zeros((6, LANES), F32)], axis=0)))
     for a in range(SIDE):
-        lanes = ends[0:2, a * LANES : (a + 1) * LANES]
+        lanes = ends[1:2, a * LANES : (a + 1) * LANES]
         for b in range(SIDE):
             snd_t[a * SIDE + b] = lanes
     spread_out(snd_t, rcv_t, 0)
 
     px = project(wx, total)
-    cx_in = shaped(
-        px[rows + PAD :], px[rows + 2 : rows + 3], px[rows + 3 : rows + 4], conv_x
-    ).astype(F32)
     pb = project(wb, total)
-    cb_in = shaped(pb[rows + PAD :], pb[rows + 2 : rows + 3], pb[rows + 3 : rows + 4], conv_b)
-    c_moved = moved(cx_in, c_steps)
-    c_scaled = (c_moved.astype(F32) * expand(jnp.exp(c_ends - c_sums))).astype(BF16)
-    tiles(snd_c, dot(cb_in, c_scaled, ((0,), (0,))))
-    spread_out(snd_c, rcv_c, 1)
-
     x_in = shaped(px[0:rows], px[rows : rows + 1], px[rows + 1 : rows + 2], conv_x).astype(F32)
     b_in = shaped(pb[0:rows], pb[rows : rows + 1], pb[rows + 1 : rows + 2], conv_b)
     l_moved = moved(x_in, l_steps)
     l_scaled = (l_moved.astype(F32) * expand(jnp.exp(l_ends - l_sums))).astype(BF16)
     tiles(snd_l, dot(b_in, l_scaled, ((0,), (0,))))
-    spread_out(snd_l, rcv_l, 2)
+    spread_out(snd_l, rcv_l, 1)
+
+    c_edges = (z > 0, z < SIDE - 1)
+    cx_in = shaped(
+        px[rows + PAD :], px[rows + 2 : rows + 3], px[rows + 3 : rows + 4], conv_x, *c_edges
+    ).astype(F32)
+    cb_in = shaped(pb[rows + PAD :], pb[rows + 2 : rows + 3], pb[rows + 3 : rows + 4], conv_b, *c_edges)
+    c_moved = moved(cx_in, c_steps)
+    c_scaled = (c_moved.astype(F32) * expand(jnp.exp(c_ends - c_sums))).astype(BF16)
+    c_full[...] = dot(cb_in, c_scaled, ((0,), (0,)))
+    c_rows = c_full[pl.ds(pl.multiple_of(y * TILE, TILE), TILE)]
+    for a in range(SIDE):
+        cut = slice(a * LANES, (a + 1) * LANES)
+        snd_c[a, 0:TILE] = c_rows[:, cut]
+        snd_c[a, TILE : TILE + 8] = jnp.broadcast_to(ends[0:1, cut], (8, LANES))
+    for k in range(1, SIDE):
+        to = lax.rem(z + k, SIDE)
+        remote(snd_c.at[to], rcv_c.at[z], line_send.at[2], line_recv.at[2], sp=on_z(k)).start()
+    rcv_c[z] = snd_c[z]
 
     pc = project(wc, rows + PAD)
     c_in = shaped(pc[0:rows], pc[rows : rows + 1], pc[rows + 1 : rows + 2], conv_c)
@@ -463,28 +494,25 @@
 
     forward = z < SIDE // 2
 
-    def place(j):
-        return jnp.where(forward, j, n_sp - 1 - j)
+    def place(j, count=n_sp):
+        return jnp.where(forward, j, count - 1 - j)
 
     all_in(rcv_t, 0)
-    all_in(rcv_c, 1)
+    line_wait(rcv_c.at[pl.ds(0, SIDE - 1)], 2)
     state = jnp.zeros((TILE, LANES), F32)
-
-    def context_step(j, state):
-        i = place(j)
-        return state * rcv_t[i, 0:1] + rcv_c[i].astype(F32)
-
-    state = lax.fori_loop(0, n_sp, context_step, state, unroll=8)
-    all_in(rcv_l, 2)
+    for j in range(SIDE):
+        i = place(j, SIDE)
+        state = state * rcv_c[i, TILE : TILE + 1] + rcv_c[i, 0:TILE]
+    all_in(rcv_l, 1)
 
     def latent_step(j, state):
         i = place(j)
         snd_b[i] = state.astype(BF16)
-        return state * rcv_t[i, 1:2] + rcv_l[i].astype(F32)
+        return state * rcv_t[i] + rcv_l[i].astype(F32)
 
     lax.fori_loop(0, n_sp, latent_step, state, unroll=8)
-    spread_out(snd_b, rcv_b, 3)
-    all_in(rcv_b, 3)
+    spread_out(snd_b, rcv_b, 2)
+    all_in(rcv_b, 2)
     entering = jnp.concatenate(
         [rcv_b[a * SIDE : (a + 1) * SIDE].reshape(STATE, LANES) for a in range(SIDE)], axis=1
     )
@@ -510,13 +538,21 @@
             o_moves.append(remote(snd_o.at[c, to], rcv_o.at[c, k], o_send.at[at], o_recv.at[at], tp=to))
             o_moves[-1].start()
 
-    for phase, sent in ((0, part_z), (1, part_y)):
+    for phase, sent in ((0, part_z), (1, part_y), (2, rcv_c.at[pl.ds(0, SIDE - 1)])):
         pltpu.make_async_copy(sent, sent, line_send.at[phase]).wait()
-    for phase, sent in ((0, rcv_t), (1, rcv_c), (2, rcv_l), (3, rcv_b)):
+    for phase, sent in ((0, rcv_t), (1, rcv_l), (2, rcv_b)):
         most = sent.at[pl.ds(0, n_sp - 1)]
         pltpu.make_async_copy(most, most, flat_send.at[phase]).wait()
-    ctx_up.wait_send()
-    ctx_down.wait_send()
+
+    @pl.when(y == SIDE - 1)
+    def _():
+        for copy in ctx_up:
+            copy.wait_send()
+
+    @pl.when(y == 0)
+    def _():
+        for copy in ctx_down:
+            copy.wait_send()
 
     @pl.when(t == n_tp - 1)
     def _():
@@ -558,7 +594,8 @@
     n_sp, n_tp, n_dp = lax.axis_size("sp"), lax.axis_size("tp"), lax.axis_size("dp")
     assert n_sp == SIDE * SIDE
     own_rows, width = latent.shape[1:]
-    ctx_rows = context.shape[1]
+    own_ctx = context.shape[1]
+    ctx_rows = SIDE * own_ctx
     cols = mod_weight.shape[2]
     inner = w_x.shape[1]
     heads = decay_rate.shape[1]
@@ -591,7 +628,7 @@
     tiles = pltpu.VMEM((n_sp, TILE, LANES), BF16)
     scratch = [pltpu.VMEM(a.shape, a.dtype) for a in args[:8]] + [
         pltpu.VMEM((n_tp, own_rows, width), BF16),
-        pltpu.VMEM((ctx_rows, width), BF16),
+        pltpu.VMEM((SIDE, own_ctx, width), BF16),
         pltpu.VMEM(mod_weight.shape, BF16),
         pltpu.VMEM((w_x.shape[0] * n_dp, inner), BF16),
         pltpu.VMEM((w_b.shape[0] * n_dp, w_b.shape[1]), BF16),
@@ -601,20 +638,21 @@
         pltpu.VMEM((w_out.shape[0] * n_dp, width), BF16),
         pltpu.VMEM((8, width), F32),
         pltpu.VMEM((4, 1, width), F32),
-        pltpu.VMEM((8, cols), F32),
-        pltpu.VMEM((SIDE - 1, 8, cols), F32),
-        pltpu.VMEM((8, cols), F32),
-        pltpu.VMEM((SIDE - 1, 8, cols), F32),
+        pltpu.VMEM((8, cols), BF16),
+        pltpu.VMEM((SIDE - 1, 8, cols), BF16),
+        pltpu.VMEM((8, cols), BF16),
+        pltpu.VMEM((SIDE - 1, 8, cols), BF16),
         pltpu.VMEM((n_tp, 8, cols), F32),
         pltpu.VMEM((4, 1, width), F32),
         pltpu.VMEM((total, width), F32),
         pltpu.VMEM((total, width), BF16),
+        pltpu.VMEM((STATE, 2 * inner), F32),
+        pltpu.VMEM((SIDE, TILE + 8, LANES), F32),
+        pltpu.VMEM((SIDE, TILE + 8, LANES), F32),
         tiles,
         tiles,
-        tiles,
-        tiles,
-        pltpu.VMEM((n_sp, 2, LANES), F32),
-        pltpu.VMEM((n_sp, 2, LANES), F32),
+        pltpu.VMEM((n_sp, 1, LANES), F32),
+        pltpu.VMEM((n_sp, 1, LANES), F32),
         tiles,
         tiles,
         pltpu.VMEM((n_tp, n_tp, own_rows, chunk), BF16),
@@ -624,20 +662,22 @@
         dma((6 * n_dp,)),
         dma((n_tp,)),
         dma((n_tp,)),
-        dma((2,)),
-        dma((2,)),
+        dma((3,)),
+        dma((3,)),
         dma((n_tp,)),
         dma((n_tp,)),
-        dma((2 + 2 * n_tp,)),
+        dma((SIDE,)),
+        dma((SIDE,)),
+        dma((2 * SIDE + 2 * n_tp,)),
         dma((4,)),
-        dma((4,)),
-        dma((4,)),
+        dma((3,)),
+        dma((3,)),
         dma((n_tp * n_tp,)),
         dma((n_tp * n_tp,)),
     ]
     result = pl.pallas_call(
         functools.partial(kernel, n_sp, n_tp, n_dp, heads),
-        out_shape=jax.ShapeDtypeStruct((own_rows, width), BF16),
+        out_shape=pltpu.VMEM((own_rows, width), BF16),
         in_specs=[anywhere] * len(args),
         out_specs=vmem,
         scratch_shapes=scratch,

time: 62.1 us -> 59.1 us (0.952)
  the two profiles are of different devices: /device:TPU:8 before, /device:TPU:16 now
where the time goes in v2:
time: 59.1 us; the launch traced here: 58.9 us
  Pallas kernels  58.2 us (98%)
  local copies, waits for them, and re-layouts  0.66 us (1%)
    pallas_call x1, Pallas kernels, shards(): pl.pallas_call(functools.partial(kernel, n_sp, n_tp, n_dp, heads), out_sh...  58.2 us

profile of v2, /device:TPU:16, one launch (start us, length us, event | category | flops | bytes accessed | tf_op | source)
XLA Modules:
  0.0 58.9 jit_solution(4094999516712151229)
XLA Ops:
  0.0 58.2 %shard_map.163 = bf16[32,2048]{1,0:T(8,128)(2,1)S(1)} custom-call(bf16[1,2048]{1,0:T(2,128)(2,1)} %condition_in.1, bf16[2048]{0:T(1024)(128)(2,1)} %source_in.1, bf16[2048]{0:T(1024)(128)(2,1)} %gain_in.1, bf16[3,512]{1,0:T(4,128)(2,1)} %conv_x_in.1, bf16[3,128]{1,0:T(4,128)(2,1)} %conv_b_in.1, bf16[3,128]{1,0:T(4,128)(2,1)} %conv_c_in.1, f32[2,8]{1,0:T(2,128)} %rate_in.1, ...), custom_call_target="tpu_custom_call" | custom-call | tf_op jit(solution)/shard_map/pallas_call | solution.py:678
  58.2 0.7 %copy.19 = bf16[1,32,2048]{2,1,0:T(8,128)(2,1)} copy(bf16[1,32,2048]{2,1,0:T(8,128)(2,1)S(1)} %bitcast.4) | data formatting | bytes 262144

commit v3 on v2

--- a/solution.py
+++ b/solution.py
@@ -103,23 +103,16 @@
     rcv_b,
     snd_o,
     rcv_o,
+    weights_like,
     local_sem,
-    dp_send,
-    dp_recv,
-    lat_send,
-    lat_recv,
+    weight_sem,
+    pack_sem,
     line_send,
     line_recv,
-    mod_send,
-    mod_recv,
-    ctx_send,
-    ctx_recv,
-    edge_send,
-    edge_recv,
+    edge_sem,
     flat_send,
     flat_recv,
-    o_send,
-    o_recv,
+    o_sem,
 ):
     s = lax.axis_index("sp")
     t = lax.axis_index("tp")
@@ -174,6 +167,9 @@
         local.append(copy)
         return copy
 
+    def settle(ref, sem):
+        pltpu.make_async_copy(ref, ref, sem).wait()
+
     early = [fetch(condition_in, condition), fetch(source_in, source), fetch(mod_weight, mod_buf)]
     lat_copy = fetch(latent, lat_all.at[t])
     ctx_copy = fetch(context, ctx_buf.at[y])
@@ -190,11 +186,10 @@
     ]
     pairs = ((w_x, wx), (w_b, wb), (w_dt, wd), (w_c, wc), (w_z, wz), (w_out, wo))
     places = []
-    weight_copies = []
     for src, dst in pairs:
         count = src.shape[0]
         places.append(dst.at[d] if src is w_dt else dst.at[pl.ds(d * count, count)])
-        weight_copies.append(fetch(src, places[-1]))
+        pltpu.make_async_copy(src, places[-1], weight_sem.at[0]).start()
 
     for copy in early:
         copy.wait()
@@ -209,8 +204,19 @@
     own_acts = own_acts.astype(BF16)
     pieces = [dot(own_acts, mod_buf[k])[0:2] for k in range(mod_buf.shape[0])]
     cols = pieces[0].shape[1]
+
+    def packed(rows_f32):
+        low = [rows_f32[r : r + 1] - rows_f32[r : r + 1].astype(BF16).astype(F32) for r in (0, 2, 4)]
+        return jnp.concatenate([rows_f32[0:5]] + low, axis=0).astype(BF16)
+
+    def unpacked(total):
+        fine = [total[r : r + 1] + total[5 + r // 2 : 6 + r // 2] for r in (0, 2, 4)]
+        return jnp.concatenate(
+            [fine[0], total[1:2], fine[1], total[3:4], fine[2], jnp.zeros((3, cols), F32)], axis=0
+        )
+
     partial = jnp.concatenate(pieces + [jnp.zeros((2, cols), F32)], axis=0)
-    part[...] = partial.astype(BF16)
+    part[...] = packed(partial)
 
     lat_copy.wait()
     edges[0] = lat_all[t, 0:1].astype(F32)
@@ -232,28 +238,21 @@
         pltpu.make_async_copy(dst, dst, line_recv.at[phase]).wait()
 
     line(part, part_z, on_z, 0)
-    lat_moves = []
     for k in range(1, n_tp):
-        lat_moves.append(
-            remote(latent, lat_all.at[t], lat_send.at[k], lat_recv.at[k], tp=lax.rem(t + k, n_tp))
-        )
-        lat_moves[-1].start()
-    for k in range(1, SIDE):
-        remote(context, ctx_buf.at[y], ctx_send.at[k], ctx_recv.at[k], sp=on_y(k)).start()
+        remote(latent, lat_all.at[t], pack_sem.at[0], pack_sem.at[1], tp=lax.rem(t + k, n_tp)).start()
     ctx_up = [
-        remote(edges.at[3], halo.at[2], edge_send.at[j], edge_recv.at[2], sp=z_up + j) for j in range(SIDE)
+        remote(edges.at[3], halo.at[2], edge_sem.at[0], edge_sem.at[4], sp=z_up + j) for j in range(SIDE)
     ]
     ctx_down = [
-        remote(edges.at[2], halo.at[3], edge_send.at[SIDE + j], edge_recv.at[3], sp=z_down + j)
+        remote(edges.at[2], halo.at[3], edge_sem.at[1], edge_sem.at[4], sp=z_down + j)
         for j in range(SIDE)
     ]
-    first = 2 * SIDE
     lat_up = [
-        remote(edges.at[1], halo.at[0], edge_send.at[first + u], edge_recv.at[0], sp=up, tp=u)
+        remote(edges.at[1], halo.at[0], edge_sem.at[2], edge_sem.at[4], sp=up, tp=u)
         for u in range(n_tp)
     ]
     lat_down = [
-        remote(edges.at[0], halo.at[1], edge_send.at[first + n_tp + u], edge_recv.at[1], sp=down, tp=u)
+        remote(edges.at[0], halo.at[1], edge_sem.at[3], edge_sem.at[4], sp=down, tp=u)
         for u in range(n_tp)
     ]
 
@@ -277,57 +276,45 @@
         for copy in lat_down:
             copy.start()
 
-    weight_moves = []
     for i, (src, dst) in enumerate(pairs):
-        for k in range(1, n_dp):
-            at = i * n_dp + k
-            weight_moves.append(
-                remote(src, places[i], dp_send.at[at], dp_recv.at[at], dp=lax.rem(d + k, n_dp))
-            )
-            weight_moves[-1].start()
+        remote(src, places[i], weight_sem.at[1], weight_sem.at[2], dp=1 - d).start()
 
     def normed(v):
         return v * lax.rsqrt(jnp.mean(v * v, axis=1, keepdims=True) + EPSILON)
 
     line_wait(part_z, 0)
-    summed = partial
+    others = part_z[0].astype(F32)
+    for k in range(2, SIDE):
+        others = others + part_z[k - 1].astype(F32)
+    summed = partial + unpacked(others)
+    part_up[...] = packed(summed)
+    line(part_up, part_y, on_y, 1)
     for k in range(1, SIDE):
-        summed = summed + part_z[k - 1].astype(F32)
-    part_up[...] = summed.astype(BF16)
-    line(part_up, part_y, on_y, 1)
-
-    for copy in lat_moves:
-        copy.wait()
+        remote(ctx_buf.at[y], ctx_buf.at[y], pack_sem.at[2], pack_sem.at[3], sp=on_y(k)).start()
+
+    line_wait(part_y, 1)
+    others = part_y[0].astype(F32)
+    for k in range(2, SIDE):
+        others = others + part_y[k - 1].astype(F32)
+    mods[t] = summed + unpacked(others)
+    for k in range(1, n_tp):
+        remote(mods.at[t], mods.at[t], pack_sem.at[4], pack_sem.at[5], tp=lax.rem(t + k, n_tp)).start()
+    settle(lat_all.at[pl.ds(0, n_tp - 1)], pack_sem.at[1])
     for u in range(n_tp):
         pre[u * own_rows : (u + 1) * own_rows] = normed(lat_all[u].astype(F32))
-    for k in range(1, SIDE):
-        remote(context, ctx_buf.at[y], ctx_send.at[k], ctx_recv.at[k], sp=on_y(k)).wait()
+    settle(ctx_buf.at[pl.ds(0, SIDE - 1)], pack_sem.at[3])
     for j in range(0, SIDE, 2):
         pre[rows + PAD + j * own_ctx : rows + PAD + (j + 2) * own_ctx] = normed(
             ctx_buf[j : j + 2].astype(F32).reshape(2 * own_ctx, width)
         )
-    ctx_up[0].wait_recv()
-    ctx_down[0].wait_recv()
-    lat_up[0].wait_recv()
-    lat_down[0].wait_recv()
+    settle(halo, edge_sem.at[4])
     pre[rows : rows + PAD] = normed(
         jnp.concatenate([halo[0], halo[1], halo[2], halo[3], jnp.zeros((PAD - 4, width), F32)], axis=0)
     )
 
-    line_wait(part_y, 1)
-    for k in range(1, SIDE):
-        summed = summed + part_y[k - 1].astype(F32)
-    mods[t] = summed
-    moves = []
-    for k in range(1, n_tp):
-        moves.append(
-            remote(mods.at[t], mods.at[t], mod_send.at[k], mod_recv.at[k], tp=lax.rem(t + k, n_tp))
-        )
-        moves[-1].start()
     for copy in small:
         copy.wait()
-    for copy in moves:
-        copy.wait()
+    settle(mods.at[pl.ds(0, n_tp - 1)], pack_sem.at[5])
 
     def vector(row):
         return jnp.concatenate([mods[c][row : row + 1] for c in range(n_tp)], axis=1)
@@ -347,10 +334,8 @@
     hid[rows + PAD : rows + PAD + ctx_rows] = (
         pre[rows + PAD : rows + PAD + ctx_rows] * ctx_gain + ctx_shift
     ).astype(BF16)
-    for copy in weight_moves:
-        copy.wait()
-    for copy in weight_copies:
-        copy.wait()
+    settle(weights_like, weight_sem.at[0])
+    settle(weights_like, weight_sem.at[2])
 
     def shaped(values, before, after, taps, has_before=s > 0, has_after=s < n_sp - 1):
         count = values.shape[0]
@@ -380,16 +365,19 @@
     def running(steps):
         count = steps.shape[0]
         logs = -rates * steps
-        a = lax.broadcasted_iota(jnp.int32, (count, count), 0)
-        b = lax.broadcasted_iota(jnp.int32, (count, count), 1)
-        lower = jnp.where(a >= b, 1.0, 0.0)
-        upper = jnp.where(a <= b, 1.0, 0.0)
-        lane = lax.broadcasted_iota(jnp.int32, logs.shape, 1)
-        sums = jnp.where(
-            lane < heads,
-            dot(lower, logs, precision=lax.Precision.HIGHEST),
-            dot(upper, logs, precision=lax.Precision.HIGHEST),
-        )
+        high = logs.astype(BF16).astype(F32)
+        rest = logs - high
+        middle = rest.astype(BF16).astype(F32)
+        low = rest - middle
+        packed = high + pltpu.roll(middle, nh2, 1) + pltpu.roll(low, 2 * nh2, 1)
+        a = lax.broadcasted_iota(jnp.int32, (2 * count, count), 0)
+        b = lax.broadcasted_iota(jnp.int32, (2 * count, count), 1)
+        keep = jnp.where(a < count, jnp.where(a >= b, 1.0, 0.0), jnp.where(a - count <= b, 1.0, 0.0))
+        parts = dot(keep.astype(BF16), packed.astype(BF16))
+        lane = lax.broadcasted_iota(jnp.int32, (count, LANES), 1)
+        parts = jnp.where(lax.rem(lane, nh2) < heads, parts[0:count], parts[count:])
+        sums = parts + pltpu.roll(parts, LANES - nh2, 1) + pltpu.roll(parts, LANES - 2 * nh2, 1)
+        sums = jnp.where(lane < nh2, sums, 0.0)
         row_lane = lax.broadcasted_iota(jnp.int32, (1, LANES), 1)
         ends = jnp.where(row_lane < heads, sums[count - 1 : count], sums[0:1])
         return sums, ends
@@ -434,8 +422,6 @@
         lanes = ends[1:2, a * LANES : (a + 1) * LANES]
         for b in range(SIDE):
             snd_t[a * SIDE + b] = lanes
-    spread_out(snd_t, rcv_t, 0)
-
     px = project(wx, total)
     pb = project(wb, total)
     x_in = shaped(px[0:rows], px[rows : rows + 1], px[rows + 1 : rows + 2], conv_x).astype(F32)
@@ -444,6 +430,7 @@
     l_scaled = (l_moved.astype(F32) * expand(jnp.exp(l_ends - l_sums))).astype(BF16)
     tiles(snd_l, dot(b_in, l_scaled, ((0,), (0,))))
     spread_out(snd_l, rcv_l, 1)
+    spread_out(snd_t, rcv_t, 0)
 
     c_edges = (z > 0, z < SIDE - 1)
     cx_in = shaped(
@@ -497,12 +484,12 @@
     def place(j, count=n_sp):
         return jnp.where(forward, j, count - 1 - j)
 
-    all_in(rcv_t, 0)
     line_wait(rcv_c.at[pl.ds(0, SIDE - 1)], 2)
     state = jnp.zeros((TILE, LANES), F32)
     for j in range(SIDE):
         i = place(j, SIDE)
         state = state * rcv_c[i, TILE : TILE + 1] + rcv_c[i, 0:TILE]
+    all_in(rcv_t, 0)
     all_in(rcv_l, 1)
 
     def latent_step(j, state):
@@ -526,50 +513,48 @@
 
     chunks = n_tp
     chunk = width // chunks
-    o_moves = []
+    far_tp = sorted(range(1, n_tp), key=lambda k: -min(k, n_tp - k))
     for c in range(chunks):
         cut = slice(c * chunk, (c + 1) * chunk)
         result = dot(ny, wo[:, cut]).astype(BF16)
         for u in range(n_tp):
             snd_o[c, u] = result[u * own_rows : (u + 1) * own_rows]
-        for k in range(1, n_tp):
+        for k in far_tp:
             to = lax.rem(t + k, n_tp)
-            at = c * n_tp + k
-            o_moves.append(remote(snd_o.at[c, to], rcv_o.at[c, k], o_send.at[at], o_recv.at[at], tp=to))
-            o_moves[-1].start()
+            remote(snd_o.at[c, to], rcv_o.at[c, k - 1], o_sem.at[chunks], o_sem.at[c], tp=to).start()
 
     for phase, sent in ((0, part_z), (1, part_y), (2, rcv_c.at[pl.ds(0, SIDE - 1)])):
-        pltpu.make_async_copy(sent, sent, line_send.at[phase]).wait()
+        settle(sent, line_send.at[phase])
     for phase, sent in ((0, rcv_t), (1, rcv_l), (2, rcv_b)):
-        most = sent.at[pl.ds(0, n_sp - 1)]
-        pltpu.make_async_copy(most, most, flat_send.at[phase]).wait()
+        settle(sent.at[pl.ds(0, n_sp - 1)], flat_send.at[phase])
+    settle(weights_like, weight_sem.at[1])
+    settle(lat_all.at[pl.ds(0, n_tp - 1)], pack_sem.at[0])
+    settle(ctx_buf.at[pl.ds(0, SIDE - 1)], pack_sem.at[2])
+    settle(mods.at[pl.ds(0, n_tp - 1)], pack_sem.at[4])
 
     @pl.when(y == SIDE - 1)
     def _():
-        for copy in ctx_up:
-            copy.wait_send()
+        settle(acts, edge_sem.at[0])
 
     @pl.when(y == 0)
     def _():
-        for copy in ctx_down:
-            copy.wait_send()
+        settle(acts, edge_sem.at[1])
 
     @pl.when(t == n_tp - 1)
     def _():
-        for copy in lat_up:
-            copy.wait_send()
+        settle(halo, edge_sem.at[2])
 
     @pl.when(t == 0)
     def _():
-        for copy in lat_down:
-            copy.wait_send()
+        settle(halo, edge_sem.at[3])
 
     for c in range(chunks):
         mixed = snd_o[c, t].astype(F32)
+        settle(rcv_o.at[c], o_sem.at[c])
         for k in range(1, n_tp):
-            o_moves[c * (n_tp - 1) + k - 1].wait()
-            mixed = mixed + rcv_o[c, k].astype(F32)
+            mixed = mixed + rcv_o[c, k - 1].astype(F32)
         out[:, c * chunk : (c + 1) * chunk] = (mods[c][4:5] * mixed).astype(BF16)
+    settle(rcv_o, o_sem.at[chunks])
 
 
 def shards(
@@ -626,6 +611,7 @@
         w_out,
     )
     tiles = pltpu.VMEM((n_sp, TILE, LANES), BF16)
+    sent_rows = sum(w.size for w in (w_x, w_b, w_c, w_dt, w_z, w_out)) // width
     scratch = [pltpu.VMEM(a.shape, a.dtype) for a in args[:8]] + [
         pltpu.VMEM((n_tp, own_rows, width), BF16),
         pltpu.VMEM((SIDE, own_ctx, width), BF16),
@@ -656,24 +642,17 @@
         tiles,
         tiles,
         pltpu.VMEM((n_tp, n_tp, own_rows, chunk), BF16),
-        pltpu.VMEM((n_tp, n_tp, own_rows, chunk), BF16),
-        dma((17,)),
-        dma((6 * n_dp,)),
-        dma((6 * n_dp,)),
-        dma((n_tp,)),
-        dma((n_tp,)),
+        pltpu.VMEM((n_tp, n_tp - 1, own_rows, chunk), BF16),
+        pltpu.VMEM((sent_rows, width), BF16),
+        dma((11,)),
+        dma((3,)),
+        dma((6,)),
         dma((3,)),
         dma((3,)),
-        dma((n_tp,)),
-        dma((n_tp,)),
-        dma((SIDE,)),
-        dma((SIDE,)),
-        dma((2 * SIDE + 2 * n_tp,)),
-        dma((4,)),
+        dma((5,)),
         dma((3,)),
         dma((3,)),
-        dma((n_tp * n_tp,)),
-        dma((n_tp * n_tp,)),
+        dma((n_tp + 1,)),
     ]
     result = pl.pallas_call(
         functools.partial(kernel, n_sp, n_tp, n_dp, heads),

time: 59.1 us -> 59.8 us (1.012)
  the two profiles are of different devices: /device:TPU:16 before, /device:TPU:1 now
where the time goes in v3:
time: 59.8 us; the launch traced here: 59.7 us
  Pallas kernels  59 us (99%)
  local copies, waits for them, and re-layouts  0.66 us (1%)
    pallas_call x1, Pallas kernels, shards(): pl.pallas_call(functools.partial(kernel, n_sp, n_tp, n_dp, heads), out_sh...  59 us

profile of v3, /device:TPU:1, one launch (start us, length us, event | category | flops | bytes accessed | tf_op | source)
XLA Modules:
  0.0 59.7 jit_solution(5738316795120362512)
XLA Ops:
  0.0 59.0 %shard_map.163 = bf16[32,2048]{1,0:T(8,128)(2,1)S(1)} custom-call(bf16[1,2048]{1,0:T(2,128)(2,1)} %condition_in.1, bf16[2048]{0:T(1024)(128)(2,1)} %source_in.1, bf16[2048]{0:T(1024)(128)(2,1)} %gain_in.1, bf16[3,512]{1,0:T(4,128)(2,1)} %conv_x_in.1, bf16[3,128]{1,0:T(4,128)(2,1)} %conv_b_in.1, bf16[3,128]{1,0:T(4,128)(2,1)} %conv_c_in.1, f32[2,8]{1,0:T(2,128)} %rate_in.1, ...), custom_call_target="tpu_custom_call" | custom-call | tf_op jit(solution)/shard_map/pallas_call | solution.py:657
  59.0 0.7 %copy.19 = bf16[1,32,2048]{2,1,0:T(8,128)(2,1)} copy(bf16[1,32,2048]{2,1,0:T(8,128)(2,1)S(1)} %bitcast.4) | data formatting | bytes 262144

commit v4 on v3

--- a/solution.py
+++ b/solution.py
@@ -34,10 +34,15 @@
     return lax.dot_general(a, b, (dims, ((), ())), precision=precision, preferred_element_type=F32)
 
 
+def reach(k):
+    return min(k, SIDE - k)
+
+
+def along():
+    return sorted(range(1, SIDE), key=lambda k: -reach(k))
+
+
 def far_first():
-    def reach(k):
-        return min(k, SIDE - k)
-
     steps = [(a, b) for a in range(SIDE) for b in range(SIDE) if a or b]
     return sorted(steps, key=lambda ab: -(reach(ab[0]) + reach(ab[1])))
 
@@ -135,6 +140,15 @@
             src_ref=src, dst_ref=dst, send_sem=send, recv_sem=recv, device_id=to, device_id_type=MESH
         )
 
+    local = []
+
+    def fetch(src, dst):
+        copy = pltpu.make_async_copy(src, dst, local_sem.at[len(local)])
+        copy.start()
+        local.append(copy)
+        return copy
+
+    early = [fetch(condition_in, condition), fetch(source_in, source), fetch(mod_weight, mod_buf)]
     barrier = pltpu.get_barrier_semaphore()
 
     def greet(**to):
@@ -146,7 +160,7 @@
     def on_y(k):
         return z * SIDE + lax.rem(y + k, SIDE)
 
-    for k in range(1, SIDE):
+    for k in along():
         greet(sp=on_z(k))
         greet(sp=on_y(k))
     for k in range(1, n_tp):
@@ -154,23 +168,20 @@
     for k in range(1, n_dp):
         greet(dp=lax.rem(d + k, n_dp))
     z_up, z_down = lax.rem(z + 1, SIDE) * SIDE, lax.rem(z + SIDE - 1, SIDE) * SIDE
-    greet(sp=z_down + SIDE - 1)
-    greet(sp=z_up)
-    greet(sp=down, tp=n_tp - 1)
-    greet(sp=up, tp=0)
-
-    local = []
-
-    def fetch(src, dst):
-        copy = pltpu.make_async_copy(src, dst, local_sem.at[len(local)])
-        copy.start()
-        local.append(copy)
-        return copy
+    is_first, is_last = s == 0, s == n_sp - 1
+
+    @pl.when(jnp.logical_not(is_first))
+    def _():
+        greet(sp=down, tp=n_tp - 1)
+
+    @pl.when(jnp.logical_not(is_last))
+    def _():
+        greet(sp=up, tp=0)
+
 
     def settle(ref, sem):
         pltpu.make_async_copy(ref, ref, sem).wait()
 
-    early = [fetch(condition_in, condition), fetch(source_in, source), fetch(mod_weight, mod_buf)]
     lat_copy = fetch(latent, lat_all.at[t])
     ctx_copy = fetch(context, ctx_buf.at[y])
     small = [
@@ -226,25 +237,30 @@
     edges[3] = ctx_buf[y, own_ctx - 1 : own_ctx].astype(F32)
 
     expected = 2 * (SIDE - 1) + n_tp - 1 + n_dp - 1
-    expected = expected + jnp.where(y == SIDE - 1, SIDE, 0) + jnp.where(y == 0, SIDE, 0)
-    expected = expected + jnp.where(t == n_tp - 1, n_tp, 0) + jnp.where(t == 0, n_tp, 0)
+    sends_up = (t == n_tp - 1) & jnp.logical_not(is_last)
+    sends_down = (t == 0) & jnp.logical_not(is_first)
+    ctx_sends_up = (y == SIDE - 1) & (z < SIDE - 1)
+    ctx_sends_down = (y == 0) & (z > 0)
+    expected = expected + jnp.where(sends_up, n_tp, 0) + jnp.where(sends_down, n_tp, 0)
     pl.semaphore_wait(barrier, expected)
 
     def line(src, dst, place, phase):
-        for k in range(1, SIDE):
+        for k in along():
             remote(src, dst.at[k - 1], line_send.at[phase], line_recv.at[phase], sp=place(k)).start()
 
     def line_wait(dst, phase):
         pltpu.make_async_copy(dst, dst, line_recv.at[phase]).wait()
 
     line(part, part_z, on_z, 0)
+    for k in along():
+        remote(ctx_buf.at[y], ctx_buf.at[y], pack_sem.at[2], pack_sem.at[3], sp=on_y(k)).start()
     for k in range(1, n_tp):
         remote(latent, lat_all.at[t], pack_sem.at[0], pack_sem.at[1], tp=lax.rem(t + k, n_tp)).start()
     ctx_up = [
-        remote(edges.at[3], halo.at[2], edge_sem.at[0], edge_sem.at[4], sp=z_up + j) for j in range(SIDE)
+        remote(edges.at[3], halo.at[2], edge_sem.at[0], edge_sem.at[6], sp=z_up + j) for j in range(SIDE)
     ]
     ctx_down = [
-        remote(edges.at[2], halo.at[3], edge_sem.at[1], edge_sem.at[4], sp=z_down + j)
+        remote(edges.at[2], halo.at[3], edge_sem.at[1], edge_sem.at[7], sp=z_down + j)
         for j in range(SIDE)
     ]
     lat_up = [
@@ -252,26 +268,16 @@
         for u in range(n_tp)
     ]
     lat_down = [
-        remote(edges.at[0], halo.at[1], edge_sem.at[3], edge_sem.at[4], sp=down, tp=u)
+        remote(edges.at[0], halo.at[1], edge_sem.at[3], edge_sem.at[5], sp=down, tp=u)
         for u in range(n_tp)
     ]
 
-    @pl.when(y == SIDE - 1)
-    def _():
-        for copy in ctx_up:
-            copy.start()
-
-    @pl.when(y == 0)
-    def _():
-        for copy in ctx_down:
-            copy.start()
-
-    @pl.when(t == n_tp - 1)
+    @pl.when(sends_up)
     def _():
         for copy in lat_up:
             copy.start()
 
-    @pl.when(t == 0)
+    @pl.when(sends_down)
     def _():
         for copy in lat_down:
             copy.start()
@@ -289,8 +295,17 @@
     summed = partial + unpacked(others)
     part_up[...] = packed(summed)
     line(part_up, part_y, on_y, 1)
-    for k in range(1, SIDE):
-        remote(ctx_buf.at[y], ctx_buf.at[y], pack_sem.at[2], pack_sem.at[3], sp=on_y(k)).start()
+
+    @pl.when(ctx_sends_up)
+    def _():
+        for copy in ctx_up:
+            copy.start()
+
+    @pl.when(ctx_sends_down)
+    def _():
+        for copy in ctx_down:
+            copy.start()
+
 
     line_wait(part_y, 1)
     others = part_y[0].astype(F32)
@@ -307,7 +322,17 @@
         pre[rows + PAD + j * own_ctx : rows + PAD + (j + 2) * own_ctx] = normed(
             ctx_buf[j : j + 2].astype(F32).reshape(2 * own_ctx, width)
         )
-    settle(halo, edge_sem.at[4])
+    inner_edges = (jnp.logical_not(is_first), jnp.logical_not(is_last), z > 0, z < SIDE - 1)
+    for j, inside_edge in enumerate(inner_edges):
+
+        @pl.when(inside_edge)
+        def _():
+            settle(halo.at[j], edge_sem.at[4 + j])
+
+        @pl.when(jnp.logical_not(inside_edge))
+        def _():
+            halo[j] = jnp.zeros((1, width), F32)
+
     pre[rows : rows + PAD] = normed(
         jnp.concatenate([halo[0], halo[1], halo[2], halo[3], jnp.zeros((PAD - 4, width), F32)], axis=0)
     )
@@ -445,7 +470,7 @@
         cut = slice(a * LANES, (a + 1) * LANES)
         snd_c[a, 0:TILE] = c_rows[:, cut]
         snd_c[a, TILE : TILE + 8] = jnp.broadcast_to(ends[0:1, cut], (8, LANES))
-    for k in range(1, SIDE):
+    for k in along():
         to = lax.rem(z + k, SIDE)
         remote(snd_c.at[to], rcv_c.at[z], line_send.at[2], line_recv.at[2], sp=on_z(k)).start()
     rcv_c[z] = snd_c[z]
@@ -498,7 +523,17 @@
         return state * rcv_t[i] + rcv_l[i].astype(F32)
 
     lax.fori_loop(0, n_sp, latent_step, state, unroll=8)
-    spread_out(snd_b, rcv_b, 2)
+    for row in range(SIDE):
+        for b in along():
+            to = row * SIDE + lax.rem(y + b, SIDE)
+            remote(snd_b.at[to], rcv_b.at[s], flat_send.at[2], flat_recv.at[2], sp=to).start()
+
+        @pl.when(z != row)
+        def _():
+            to = row * SIDE + y
+            remote(snd_b.at[to], rcv_b.at[s], flat_send.at[2], flat_recv.at[2], sp=to).start()
+
+    rcv_b[s] = snd_b[s]
     all_in(rcv_b, 2)
     entering = jnp.concatenate(
         [rcv_b[a * SIDE : (a + 1) * SIDE].reshape(STATE, LANES) for a in range(SIDE)], axis=1
@@ -532,21 +567,14 @@
     settle(ctx_buf.at[pl.ds(0, SIDE - 1)], pack_sem.at[2])
     settle(mods.at[pl.ds(0, n_tp - 1)], pack_sem.at[4])
 
-    @pl.when(y == SIDE - 1)
-    def _():
-        settle(acts, edge_sem.at[0])
-
-    @pl.when(y == 0)
-    def _():
-        settle(acts, edge_sem.at[1])
-
-    @pl.when(t == n_tp - 1)
-    def _():
-        settle(halo, edge_sem.at[2])
-
-    @pl.when(t == 0)
-    def _():
-        settle(halo, edge_sem.at[3])
+    for j, (ref, sends) in enumerate(
+        ((acts, ctx_sends_up), (acts, ctx_sends_down), (halo, sends_up), (halo, sends_down))
+    ):
+
+        @pl.when(sends)
+        def _():
+            settle(ref, edge_sem.at[j])
+
 
     for c in range(chunks):
         mixed = snd_o[c, t].astype(F32)
@@ -649,7 +677,7 @@
         dma((6,)),
         dma((3,)),
         dma((3,)),
-        dma((5,)),
+        dma((8,)),
         dma((3,)),
         dma((3,)),
         dma((n_tp + 1,)),

time: 59.8 us -> 56.3 us (0.941)
  the two profiles are of different devices: /device:TPU:1 before, /device:TPU:128 now
where the time goes in v4:
time: 56.3 us; the launch traced here: 56.2 us
  Pallas kernels  55.5 us (99%)
  local copies, waits for them, and re-layouts  0.66 us (1%)
    pallas_call x1, Pallas kernels, shards(): pl.pallas_call(functools.partial(kernel, n_sp, n_tp, n_dp, heads), out_sh...  55.5 us

profile of v4, /device:TPU:128, one launch (start us, length us, event | category | flops | bytes accessed | tf_op | source)
XLA Modules:
  0.0 56.2 jit_solution(12365961442670626716)
XLA Ops:
  0.0 55.5 %shard_map.163 = bf16[32,2048]{1,0:T(8,128)(2,1)S(1)} custom-call(bf16[1,2048]{1,0:T(2,128)(2,1)} %condition_in.1, bf16[2048]{0:T(1024)(128)(2,1)} %source_in.1, bf16[2048]{0:T(1024)(128)(2,1)} %gain_in.1, bf16[3,512]{1,0:T(4,128)(2,1)} %conv_x_in.1, bf16[3,128]{1,0:T(4,128)(2,1)} %conv_b_in.1, bf16[3,128]{1,0:T(4,128)(2,1)} %conv_c_in.1, f32[2,8]{1,0:T(2,128)} %rate_in.1, ...), custom_call_target="tpu_custom_call" | custom-call | tf_op jit(solution)/shard_map/pallas_call | solution.py:685
  55.5 0.7 %copy.19 = bf16[1,32,2048]{2,1,0:T(8,128)(2,1)} copy(bf16[1,32,2048]{2,1,0:T(8,128)(2,1)S(1)} %bitcast.4) | data formatting | bytes 262144

commit v5 on v4

--- a/solution.py
+++ b/solution.py
@@ -356,9 +356,6 @@
     hid[rows : rows + PAD] = jnp.where(
         at_row < 2, edge * lat_gain + lat_shift, edge * ctx_gain + ctx_shift
     ).astype(BF16)
-    hid[rows + PAD : rows + PAD + ctx_rows] = (
-        pre[rows + PAD : rows + PAD + ctx_rows] * ctx_gain + ctx_shift
-    ).astype(BF16)
     settle(weights_like, weight_sem.at[0])
     settle(weights_like, weight_sem.at[2])
 
@@ -372,10 +369,11 @@
         w = taps[...].astype(F32)
         return silu(earlier * w[0:1] + values * w[1:2] + later * w[2:3]).astype(BF16)
 
-    def project(weight, count):
-        return dot(hid[0:count], weight[...]).astype(BF16).astype(F32)
+    def project(weight, first, last):
+        return dot(hid[first:last], weight[...]).astype(BF16).astype(F32)
 
     total = rows + PAD + ctx_rows
+    half = wd.shape[3]
     spread_at = lax.broadcasted_iota(jnp.int32, (LANES, both), 0)
     spread_to = lax.broadcasted_iota(jnp.int32, (LANES, both), 1) // head_dim
     spreader = jnp.where((spread_to == spread_at) | (spread_to + nh2 == spread_at), 1.0, 0.0).astype(BF16)
@@ -428,54 +426,66 @@
                     b * TILE : (b + 1) * TILE, a * LANES : (a + 1) * LANES
                 ].astype(BF16)
 
-    features = None
-    half = wd.shape[3]
-    for r in range(n_dp):
-        taps = jnp.concatenate(
+    dt_taps = [
+        jnp.concatenate(
             [wd[r, 0].astype(F32), wd[r, 1].astype(F32), jnp.zeros((LANES - nh2, half), F32)], axis=0
         ).astype(BF16)
-        one = dot(hid[0:total, r * half : (r + 1) * half], taps, ((1,), (1,)))
-        features = one if features is None else features + one
-    step_all = softplus(features.astype(BF16).astype(F32))
+        for r in range(n_dp)
+    ]
+
+    def steps_of(first, last):
+        features = None
+        for r in range(n_dp):
+            one = dot(hid[first:last, r * half : (r + 1) * half], dt_taps[r], ((1,), (1,)))
+            features = one if features is None else features + one
+        return softplus(features.astype(BF16).astype(F32))
+
     rates = jnp.concatenate([rate[0:1], rate[1:2], jnp.zeros((1, LANES - nh2), F32)], axis=1)
-    c_steps = step_all[rows + PAD :]
-    c_sums, c_ends = running(c_steps)
-    l_steps = step_all[0:rows]
+    l_steps = steps_of(0, rows)
     l_sums, l_ends = running(l_steps)
-    ends = expand(jnp.exp(jnp.concatenate([c_ends, l_ends, jnp.zeros((6, LANES), F32)], axis=0)))
+    ends = expand(jnp.exp(jnp.broadcast_to(l_ends, (8, LANES))))
     for a in range(SIDE):
-        lanes = ends[1:2, a * LANES : (a + 1) * LANES]
-        for b in range(SIDE):
-            snd_t[a * SIDE + b] = lanes
-    px = project(wx, total)
-    pb = project(wb, total)
+        snd_t[a] = ends[0:1, a * LANES : (a + 1) * LANES]
+    px = project(wx, 0, rows + PAD)
+    pb = project(wb, 0, rows + PAD)
     x_in = shaped(px[0:rows], px[rows : rows + 1], px[rows + 1 : rows + 2], conv_x).astype(F32)
     b_in = shaped(pb[0:rows], pb[rows : rows + 1], pb[rows + 1 : rows + 2], conv_b)
     l_moved = moved(x_in, l_steps)
     l_scaled = (l_moved.astype(F32) * expand(jnp.exp(l_ends - l_sums))).astype(BF16)
     tiles(snd_l, dot(b_in, l_scaled, ((0,), (0,))))
-    spread_out(snd_l, rcv_l, 1)
-    spread_out(snd_t, rcv_t, 0)
-
+    spread_out(snd_l, rcv_l, 0)
+    for a, b in far_first():
+        row = lax.rem(z + a, SIDE)
+        to = row * SIDE + lax.rem(y + b, SIDE)
+        remote(snd_t.at[row], rcv_t.at[s], flat_send.at[2], flat_recv.at[2], sp=to).start()
+    rcv_t[s] = snd_t[z]
+
+    hid[rows + PAD : rows + PAD + ctx_rows] = (
+        pre[rows + PAD : rows + PAD + ctx_rows] * ctx_gain + ctx_shift
+    ).astype(BF16)
+    c_steps = steps_of(rows + PAD, total)
+    c_sums, c_ends = running(c_steps)
+    c_decay = expand(jnp.exp(jnp.broadcast_to(c_ends, (8, LANES))))
+    cpx = project(wx, rows, total)
+    cpb = project(wb, rows, total)
     c_edges = (z > 0, z < SIDE - 1)
-    cx_in = shaped(
-        px[rows + PAD :], px[rows + 2 : rows + 3], px[rows + 3 : rows + 4], conv_x, *c_edges
-    ).astype(F32)
-    cb_in = shaped(pb[rows + PAD :], pb[rows + 2 : rows + 3], pb[rows + 3 : rows + 4], conv_b, *c_edges)
+    cx_in = shaped(cpx[PAD:], cpx[2:3], cpx[3:4], conv_x, *c_edges).astype(F32)
+    cb_in = shaped(cpb[PAD:], cpb[2:3], cpb[3:4], conv_b, *c_edges)
     c_moved = moved(cx_in, c_steps)
     c_scaled = (c_moved.astype(F32) * expand(jnp.exp(c_ends - c_sums))).astype(BF16)
     c_full[...] = dot(cb_in, c_scaled, ((0,), (0,)))
     c_rows = c_full[pl.ds(pl.multiple_of(y * TILE, TILE), TILE)]
+    c_high = c_decay.astype(BF16).astype(F32)
+    c_tail = jnp.where(lax.broadcasted_iota(jnp.int32, c_decay.shape, 0) == 0, c_high, c_decay - c_high)
+    c_all = jnp.concatenate([c_rows, c_tail], axis=0).astype(BF16)
     for a in range(SIDE):
-        cut = slice(a * LANES, (a + 1) * LANES)
-        snd_c[a, 0:TILE] = c_rows[:, cut]
-        snd_c[a, TILE : TILE + 8] = jnp.broadcast_to(ends[0:1, cut], (8, LANES))
+        snd_c[a] = c_all[:, a * LANES : (a + 1) * LANES]
     for k in along():
         to = lax.rem(z + k, SIDE)
         remote(snd_c.at[to], rcv_c.at[z], line_send.at[2], line_recv.at[2], sp=on_z(k)).start()
     rcv_c[z] = snd_c[z]
 
-    pc = project(wc, rows + PAD)
+    pc = project(wc, 0, rows + PAD)
     c_in = shaped(pc[0:rows], pc[rows : rows + 1], pc[rows + 1 : rows + 2], conv_c)
     scores = dot(c_in, b_in, ((1,), (1,)))
     at_t = lax.broadcasted_iota(jnp.int32, (rows, rows), 0)
@@ -502,7 +512,7 @@
         inside.append(value)
     inside = jnp.concatenate(inside, axis=1)
     growth = expand(jnp.exp(l_sums))
-    gate = silu(project(wz, rows))
+    gate = silu(project(wz, 0, rows))
 
     forward = z < SIDE // 2
 
@@ -513,9 +523,10 @@
     state = jnp.zeros((TILE, LANES), F32)
     for j in range(SIDE):
         i = place(j, SIDE)
-        state = state * rcv_c[i, TILE : TILE + 1] + rcv_c[i, 0:TILE]
-    all_in(rcv_t, 0)
-    all_in(rcv_l, 1)
+        piece = rcv_c[i].astype(F32)
+        state = state * (piece[TILE : TILE + 1] + piece[TILE + 1 : TILE + 2]) + piece[0:TILE]
+    all_in(rcv_t, 2)
+    all_in(rcv_l, 0)
 
     def latent_step(j, state):
         i = place(j)
@@ -526,15 +537,15 @@
     for row in range(SIDE):
         for b in along():
             to = row * SIDE + lax.rem(y + b, SIDE)
-            remote(snd_b.at[to], rcv_b.at[s], flat_send.at[2], flat_recv.at[2], sp=to).start()
+            remote(snd_b.at[to], rcv_b.at[s], flat_send.at[1], flat_recv.at[1], sp=to).start()
 
         @pl.when(z != row)
         def _():
             to = row * SIDE + y
-            remote(snd_b.at[to], rcv_b.at[s], flat_send.at[2], flat_recv.at[2], sp=to).start()
+            remote(snd_b.at[to], rcv_b.at[s], flat_send.at[1], flat_recv.at[1], sp=to).start()
 
     rcv_b[s] = snd_b[s]
-    all_in(rcv_b, 2)
+    all_in(rcv_b, 1)
     entering = jnp.concatenate(
         [rcv_b[a * SIDE : (a + 1) * SIDE].reshape(STATE, LANES) for a in range(SIDE)], axis=1
     )
@@ -558,9 +569,10 @@
             to = lax.rem(t + k, n_tp)
             remote(snd_o.at[c, to], rcv_o.at[c, k - 1], o_sem.at[chunks], o_sem.at[c], tp=to).start()
 
-    for phase, sent in ((0, part_z), (1, part_y), (2, rcv_c.at[pl.ds(0, SIDE - 1)])):
+    most = pl.ds(0, SIDE - 1)
+    for phase, sent in enumerate((part_z, part_y, rcv_c.at[most])):
         settle(sent, line_send.at[phase])
-    for phase, sent in ((0, rcv_t), (1, rcv_l), (2, rcv_b)):
+    for phase, sent in enumerate((rcv_l, rcv_b, rcv_t)):
         settle(sent.at[pl.ds(0, n_sp - 1)], flat_send.at[phase])
     settle(weights_like, weight_sem.at[1])
     settle(lat_all.at[pl.ds(0, n_tp - 1)], pack_sem.at[0])
@@ -661,11 +673,11 @@
         pltpu.VMEM((total, width), F32),
         pltpu.VMEM((total, width), BF16),
         pltpu.VMEM((STATE, 2 * inner), F32),
-        pltpu.VMEM((SIDE, TILE + 8, LANES), F32),
-        pltpu.VMEM((SIDE, TILE + 8, LANES), F32),
+        pltpu.VMEM((SIDE, TILE + 8, LANES), BF16),
+        pltpu.VMEM((SIDE, TILE + 8, LANES), BF16),
         tiles,
         tiles,
-        pltpu.VMEM((n_sp, 1, LANES), F32),
+        pltpu.VMEM((SIDE, 1, LANES), F32),
         pltpu.VMEM((n_sp, 1, LANES), F32),
         tiles,
         tiles,

time: 56.3 us -> 54.7 us (0.972)
  the two profiles are of different devices: /device:TPU:128 before, /device:TPU:130 now
where the time goes in v5:
time: 54.7 us; the launch traced here: 54.6 us
  Pallas kernels  53.9 us (99%)
  local copies, waits for them, and re-layouts  0.66 us (1%)
    pallas_call x1, Pallas kernels, shards(): pl.pallas_call(functools.partial(kernel, n_sp, n_tp, n_dp, heads), out_sh...  53.9 us

profile of v5, /device:TPU:130, one launch (start us, length us, event | category | flops | bytes accessed | tf_op | source)
XLA Modules:
  0.0 54.6 jit_solution(9079063960182183766)
XLA Ops:
  0.0 53.9 %shard_map.163 = bf16[32,2048]{1,0:T(8,128)(2,1)S(1)} custom-call(bf16[1,2048]{1,0:T(2,128)(2,1)} %condition_in.1, bf16[2048]{0:T(1024)(128)(2,1)} %source_in.1, bf16[2048]{0:T(1024)(128)(2,1)} %gain_in.1, bf16[3,512]{1,0:T(4,128)(2,1)} %conv_x_in.1, bf16[3,128]{1,0:T(4,128)(2,1)} %conv_b_in.1, bf16[3,128]{1,0:T(4,128)(2,1)} %conv_c_in.1, f32[2,8]{1,0:T(2,128)} %rate_in.1, ...), custom_call_target="tpu_custom_call" | custom-call | tf_op jit(solution)/shard_map/pallas_call | solution.py:697
  53.9 0.7 %copy.19 = bf16[1,32,2048]{2,1,0:T(8,128)(2,1)} copy(bf16[1,32,2048]{2,1,0:T(8,128)(2,1)S(1)} %bitcast.4) | data formatting | bytes 262144

commit v6 on v5

--- a/solution.py
+++ b/solution.py
@@ -513,6 +513,8 @@
     inside = jnp.concatenate(inside, axis=1)
     growth = expand(jnp.exp(l_sums))
     gate = silu(project(wz, 0, rows))
+    inside = inside * gate
+    growth = growth * jnp.concatenate([gate, gate], axis=1)
 
     forward = z < SIDE // 2
 
@@ -550,7 +552,7 @@
         [rcv_b[a * SIDE : (a + 1) * SIDE].reshape(STATE, LANES) for a in range(SIDE)], axis=1
     )
     carried = dot(c_in, entering) * growth
-    gated = (inside + carried[:, 0:inner] + carried[:, inner:both]) * gate
+    gated = inside + carried[:, 0:inner] + carried[:, inner:both]
     ny = (
         gated
         * lax.rsqrt(jnp.mean(gated * gated, axis=1, keepdims=True) + EPSILON)

time: 54.7 us -> 54.7 us (level)
  no operation moved by 1% of the time
where the time goes in v6:
time: 54.7 us; the launch traced here: 54.6 us
  Pallas kernels  53.9 us (99%)
  local copies, waits for them, and re-layouts  0.66 us (1%)
    pallas_call x1, Pallas kernels, shards(): pl.pallas_call(functools.partial(kernel, n_sp, n_tp, n_dp, heads), out_sh...  53.9 us

profile of v6, /device:TPU:130, one launch (start us, length us, event | category | flops | bytes accessed | tf_op | source)
XLA Modules:
  0.0 54.6 jit_solution(5730870537837581546)
XLA Ops:
  0.0 53.9 %shard_map.163 = bf16[32,2048]{1,0:T(8,128)(2,1)S(1)} custom-call(bf16[1,2048]{1,0:T(2,128)(2,1)} %condition_in.1, bf16[2048]{0:T(1024)(128)(2,1)} %source_in.1, bf16[2048]{0:T(1024)(128)(2,1)} %gain_in.1, bf16[3,512]{1,0:T(4,128)(2,1)} %conv_x_in.1, bf16[3,128]{1,0:T(4,128)(2,1)} %conv_b_in.1, bf16[3,128]{1,0:T(4,128)(2,1)} %conv_c_in.1, f32[2,8]{1,0:T(2,128)} %rate_in.1, ...), custom_call_target="tpu_custom_call" | custom-call | tf_op jit(solution)/shard_map/pallas_call | solution.py:699
  53.9 0.7 %copy.19 = bf16[1,32,2048]{2,1,0:T(8,128)(2,1)} copy(bf16[1,32,2048]{2,1,0:T(8,128)(2,1)S(1)} %bitcast.4) | data formatting | bytes 262144
